TPU v7x, 512 devices: a whole 4x8x8 slice. The times are simulated.
512 devices in a mesh: sp: 128 (over z, y, core), tp: 4 (over x).
Axes of the slice: x: 4, y: 8, z: 8, core: 2. Of those that a mesh axis runs over, the one named last changes fastest.
Arguments:
- inputs: bfloat16 [2, 16384, 2048], P(None, 'sp'), may hold values from -6 to 6
- norm_gain: float32 [2048], replicated, may hold values from 0.1 to 1.9
- query_weight: bfloat16 [2048, 1024], P('sp', 'tp'), may hold values from -0.125 to 0.125
- key_weight: bfloat16 [2048, 256], P('sp', 'tp'), may hold values from -0.125 to 0.125
- value_weight: bfloat16 [2048, 256], P('sp', 'tp'), may hold values from -0.125 to 0.125
- query_gain: float32 [64], replicated, may hold values from 0.1 to 24
- key_gain: float32 [64], replicated, may hold values from 0.1 to 1.9
- forget_cache: float32 [2, 16, 16384], P(None, 'tp'), may hold values from -1640 to 0, as said below
- rec_in_weight: bfloat16 [2048, 1024], P('sp', 'tp'), may hold values from -0.125 to 0.125
- rec_gate_weight: bfloat16 [2048, 1024], P('sp', 'tp'), may hold values from -0.125 to 0.125
- conv_weight: bfloat16 [4, 1024], P(None, 'tp'), may hold values from -3 to 3
- decay_gate_weight: bfloat16 [16, 64, 64], P('tp'), may hold values from -0.75 to 0.75
- input_gate_weight: bfloat16 [16, 64, 64], P('tp'), may hold values from -0.75 to 0.75
- decay_param: float32 [1024], P('tp'), may hold values from 4 to 16
- decay_extra: float32 [2, 16384, 1024], P(None, 'sp', 'tp'), may hold values from -2 to 0
- attn_out_gain: float32 [1024], P('tp'), may hold values from 0.1 to 1.9
- rec_out_gain: float32 [1024], P('tp'), may hold values from 0.1 to 1.9
- out_att_weight: bfloat16 [1024, 2048], P('tp'), may hold values from -0.125 to 0.125
- out_rec_weight: bfloat16 [1024, 2048], P('tp'), may hold values from -0.125 to 0.125
Outputs:
- mixed: bfloat16 [2, 16384, 2048], P(None, 'sp', 'tp')
Inputs may be any that keep to these rules, and one draw needn't show every extreme that they name: `forget_cache`: Non-increasing along the positions of each sequence and head.
All inputs are finite; a program needn't handle non-finite values.
Results may differ from a plain program's by a relative error of at most 0.012.
The roundings to bfloat16 on the way count: a program that leaves them out, or rounds other values in their place, can miss the bound.
Values may be sent and summed in bfloat16 or wider, within the bound.
A program may use at most 128 MiB of HBM per device.

v0:
```python
import jax
import jax.numpy as jnp
from jax import lax
from jax.sharding import Mesh
from jax.sharding import PartitionSpec as P

D = 2048
LRU_BLOCK = 64
CONV_TAPS = 4
SP = ("sp_0", "sp_1", "sp_2")


lru_const = 8.0
norm_eps = 1e-06


def side_by_side(arrays, axis, dim, along):
    both = jnp.concatenate(arrays, axis=along)
    filled, at, finished = (lax.all_gather(both, axis, axis=dim, tiled=True), 0, [])
    for a in arrays:
        finished.append(lax.slice_in_dim(filled, at, at + a.shape[along], axis=along))
        at += a.shape[along]
    return tuple(finished)


def from_behind(value, axis, steps):
    count = lax.axis_size(axis)
    leading, last = (max(0, -steps), min(count, count - steps))
    return lax.ppermute(value, axis, [(source, source + steps) for source in range(leading, last)])


def filled_with(shard, identity):
    return jax.tree.map(
        lambda a, e: jnp.broadcast_to(jnp.asarray(e, a.dtype), a.shape), shard, identity
    )


def collected_together(shard, axis):
    leaves = jax.tree.leaves(shard)
    order = sorted(range(len(leaves)), key=lambda k: -leaves[k].size)
    width = (1, *leaves[order[0]].shape)[-1]
    lines = [
        jnp.pad(leaves[k].reshape(-1), (0, -leaves[k].size % width)).reshape(-1, width)
        for k in order
    ]
    both, at, found = (lax.all_gather(jnp.concatenate(lines), axis), 0, {})
    for k, line in zip(order, lines):
        share = both[:, at : at + len(line)].reshape(len(both), -1)
        found[k] = share[:, : leaves[k].size].reshape(-1, *leaves[k].shape)
        at += len(line)
    numbers = iter(range(len(leaves)))
    return jax.tree.map(lambda _: found[next(numbers)], shard)


def entering_2(shard, axes, combine, identity):
    before = start = filled_with(shard, identity)
    so_far = shard
    for axis in reversed(axes):
        peers, place = (lax.axis_size(axis), lax.axis_index(axis))
        pieces = collected_together(so_far, axis)
        inside, so_far = (start, start)
        for k in range(peers):
            passed = k < place
            so_far = combine(so_far, jax.tree.map(lambda part: part[k], pieces))
            inside = jax.tree.map(lambda new, old: jnp.where(passed, new, old), so_far, inside)
        before = combine(inside, before)
    return before


def in_blocks(shard, dim, peers):
    dims = shard.shape
    parts = shard.reshape(*dims[:dim], peers, dims[dim] // peers, *dims[dim + 1 :])
    return jnp.moveaxis(parts, dim, 0)


def sent_and_summed(shard, axis, dim):
    peers = lax.axis_size(axis)
    parts = lax.all_to_all(in_blocks(shard, dim, peers), axis, 0, 0, tiled=True)
    return jnp.sum(parts.astype(jnp.float32), axis=0)


def rms_scale(values, gain):
    multiplier = lax.rsqrt(jnp.mean(values * values, axis=-1, keepdims=True) + norm_eps)
    return values * multiplier * gain


def merge_state(earlier, later):
    return (earlier[0] * later[0], later[0] * earlier[1] + later[1])


def block_length(length, span):
    shards = max(length // span, 1)
    group_size = 1
    for trial_size in range(1, shards + 1):
        if shards % trial_size == 0 and trial_size * span <= 1024:
            group_size = trial_size
    sub_size = group_size * span
    if length % sub_size:
        sub_size = length
    return sub_size


def body(
    inputs,
    norm_gain,
    query_weight,
    key_weight,
    value_weight,
    query_gain,
    key_gain,
    forget_cache,
    rec_in_weight,
    rec_gate_weight,
    conv_weight,
    decay_gate_weight,
    input_gate_weight,
    decay_param,
    decay_extra,
    attn_out_gain,
    rec_out_gain,
    out_att_weight,
    out_rec_weight,
):
    seq_count, seq_span, model_width = inputs.shape
    row_count = seq_count * seq_span
    head_dim = query_gain.shape[0]
    att_local = query_weight.shape[1] // head_dim
    kv_local = key_weight.shape[1] // head_dim
    head_group = att_local // kv_local
    channels = rec_in_weight.shape[1]
    normed = rms_scale(
        inputs.reshape(row_count, model_width).astype(jnp.float32), norm_gain
    ).astype(jnp.bfloat16)
    normed_cols = normed.T
    row_contract = (((0,), (0,)), ((), ()))
    kv_cols = key_weight.shape[1]
    pieces = side_by_side(
        (query_weight, key_weight, value_weight, rec_in_weight, rec_gate_weight), SP, 0, 1
    )
    query_proj, key_proj, value_sum, rec_in_sum, gate_proj = tuple(
        (
            lax.dot_general(
                normed_cols, weight_part, row_contract, preferred_element_type=jnp.float32
            )
            for weight_part in pieces
        )
    )
    queries = rms_scale(query_proj.reshape(row_count, att_local, head_dim), query_gain).astype(
        jnp.bfloat16
    )
    queries = queries.reshape(seq_count, seq_span, kv_local, head_group, head_dim).transpose(
        0, 2, 3, 1, 4
    )
    queries = queries.reshape(seq_count, kv_local, head_group * seq_span, head_dim)
    key_heads = rms_scale(key_proj.reshape(row_count, kv_local, head_dim), key_gain).astype(
        jnp.bfloat16
    )
    key_heads = key_heads.reshape(seq_count, seq_span, kv_cols)
    value_heads = value_sum.astype(jnp.bfloat16).reshape(seq_count, seq_span, kv_cols)
    key_value = jnp.concatenate([key_heads, value_heads], axis=2)
    my_first = lax.axis_index(SP) * seq_span
    own_gates = lax.dynamic_slice_in_dim(forget_cache, my_first, seq_span, 2)
    own_gates = own_gates.reshape(seq_count, kv_local, head_group, seq_span, 1)
    query_pos = my_first + jnp.tile(jnp.arange(seq_span, dtype=jnp.int32), head_group)
    scaling = head_dim ** (-0.5)
    start_state = (
        jnp.full((seq_count, kv_local, head_group * seq_span), -jnp.inf, jnp.float32),
        jnp.zeros((seq_count, kv_local, head_group * seq_span), jnp.float32),
        jnp.zeros((seq_count, kv_local, head_group * seq_span, head_dim), jnp.float32),
    )
    shard_part = lax.all_gather(key_value, SP, axis=1, tiled=True)
    offset = jnp.int32(0)
    length = shard_part.shape[1]
    sub_size = block_length(length, seq_span)

    def one_step(block_index, carried_state):
        key_first = offset + block_index * sub_size

        def work(carried):
            top_score, totals, accum = carried
            block_rows = lax.dynamic_slice_in_dim(shard_part, block_index * sub_size, sub_size, 1)
            key_block = block_rows[:, :, :kv_cols].reshape(seq_count, sub_size, kv_local, head_dim)
            value_block = block_rows[:, :, kv_cols:].reshape(
                seq_count, sub_size, kv_local, head_dim
            )
            key_gates = lax.dynamic_slice_in_dim(forget_cache, key_first, sub_size, 2)
            key_gates = key_gates.reshape(seq_count, kv_local, head_group, 1, sub_size)
            scores = (
                jnp.einsum(
                    "bhqd,bkhd->bhqk", queries, key_block, preferred_element_type=jnp.float32
                )
                * scaling
            )
            scores = (
                scores.reshape(seq_count, kv_local, head_group, seq_span, sub_size)
                + own_gates
                - key_gates
            )
            scores = scores.reshape(seq_count, kv_local, head_group * seq_span, sub_size)
            visible = (
                query_pos[:, None] >= (key_first + jnp.arange(sub_size, dtype=jnp.int32))[None, :]
            )
            scores = jnp.where(visible, scores, -jnp.inf)
            new_top = jnp.maximum(top_score, jnp.max(scores, axis=-1))
            safe_top = jnp.where(jnp.isfinite(new_top), new_top, 0.0)
            weights = jnp.exp(scores - safe_top[..., None])
            fading = jnp.exp(top_score - safe_top)
            totals = totals * fading + jnp.sum(weights, axis=-1)
            accum = accum * fading[..., None] + jnp.einsum(
                "bhqk,bkhd->bhqd",
                weights.astype(jnp.bfloat16),
                value_block,
                preferred_element_type=jnp.float32,
            )
            return (new_top, totals, accum)

        return lax.cond(
            key_first < my_first + seq_span, work, lambda carried: carried, carried_state
        )

    top_score, totals, accum = lax.fori_loop(0, length // sub_size, one_step, start_state)
    attended = (accum / totals[..., None]).reshape(
        seq_count, kv_local, head_group, seq_span, head_dim
    )
    attended = attended.transpose(0, 3, 1, 2, 4).reshape(row_count, att_local, head_dim)
    att_normed = rms_scale(attended, attn_out_gain.reshape(att_local, head_dim)).astype(
        jnp.bfloat16
    )
    att_normed = att_normed.reshape(row_count, att_local * head_dim)
    rec_in = rec_in_sum.astype(jnp.bfloat16).reshape(seq_count, seq_span, channels)
    before = from_behind(rec_in[:, seq_span - (CONV_TAPS - 1) :, :], SP, 1)
    extended = jnp.concatenate([before, rec_in], axis=1)
    conv = jnp.zeros((seq_count, seq_span, channels), jnp.float32)
    for tap in range(CONV_TAPS):
        conv = conv + extended[:, tap : tap + seq_span].astype(jnp.float32) * conv_weight[
            tap
        ].astype(jnp.float32)
    conv = conv.astype(jnp.bfloat16)
    blocks_local = decay_gate_weight.shape[0]
    grouped = conv.reshape(seq_count, seq_span, blocks_local, LRU_BLOCK)
    gate_decay = jnp.einsum(
        "bsnd,nde->bsne", grouped, decay_gate_weight, preferred_element_type=jnp.float32
    ).reshape(seq_count, seq_span, channels)
    gate_input = jnp.einsum(
        "bsnd,nde->bsne", grouped, input_gate_weight, preferred_element_type=jnp.float32
    ).reshape(seq_count, seq_span, channels)
    log_decay = (
        -lru_const * jax.nn.sigmoid(gate_decay) * jax.nn.softplus(-decay_param) + decay_extra
    )
    drive = (
        jnp.sqrt(-jnp.expm1(2.0 * log_decay))
        * jax.nn.sigmoid(gate_input)
        * conv.astype(jnp.float32)
    )
    cum_decay, local_state = lax.associative_scan(merge_state, (jnp.exp(log_decay), drive), axis=1)
    entering = entering_2(
        (cum_decay[:, seq_span - 1], local_state[:, seq_span - 1]),
        SP,
        merge_state,
        (
            jnp.ones((seq_count, channels), jnp.float32),
            jnp.zeros((seq_count, channels), jnp.float32),
        ),
    )[1]
    state = local_state + cum_decay * entering[:, None, :]
    gated = state * jax.nn.gelu(gate_proj.reshape(seq_count, seq_span, channels))
    rec_normed = rms_scale(
        gated.reshape(row_count, blocks_local, LRU_BLOCK),
        rec_out_gain.reshape(blocks_local, LRU_BLOCK),
    ).astype(jnp.bfloat16)
    rec_normed = rec_normed.reshape(row_count, channels)
    out_cols = D // lax.axis_size("tp")
    pieces = row_count * lax.axis_size("tp") // row_count
    terms = jnp.dot(att_normed, out_att_weight, preferred_element_type=jnp.float32) + jnp.dot(
        rec_normed, out_rec_weight, preferred_element_type=jnp.float32
    )
    mixed_cols = sent_and_summed(
        terms.reshape(row_count, pieces, out_cols)
        .transpose(1, 0, 2)
        .reshape(pieces * row_count, out_cols)
        .astype(jnp.bfloat16),
        "tp",
        0,
    )
    return mixed_cols.astype(jnp.bfloat16).reshape(seq_count, seq_span, out_cols)


def solution(mesh):
    finer = Mesh(mesh.devices.reshape(8, 8, 2, mesh.shape["tp"]), ("sp_0", "sp_1", "sp_2", "tp"))
    return jax.shard_map(
        body,
        mesh=finer,
        in_specs=(
            P(None, SP, None),
            P(),
            P(SP, "tp"),
            P(SP, "tp"),
            P(SP, "tp"),
            P(),
            P(),
            P(None, "tp", None),
            P(SP, "tp"),
            P(SP, "tp"),
            P(None, "tp"),
            P("tp", None, None),
            P("tp", None, None),
            P("tp"),
            P(None, SP, "tp"),
            P("tp"),
            P("tp"),
            P("tp", None),
            P("tp", None),
        ),
        out_specs=P(None, SP, "tp"),
        check_vma=False,
    )
```

profile of v0, /device:TPU:504, one launch (start us, length us, event | category | flops | bytes accessed | tf_op | source)
XLA Modules:
  0.0 546.3 jit_solution(5996437220819198975)
XLA Ops:
  11.2 78.8 %all-gather.9.cloned.1.call-done = bf16[2048,896]{1,0:T(8,128)(2,1)} async-done(((bf16[16,896]{1,0:T(8,128)(2,1)}), bf16[2048,896]{1,0:T(8,128)(2,1)}) %all-gather.9.cloned.1.call-update) | async-done | bytes 3670032 | tf_op jit(solution)/shard_map/all_gather | solution.py:19
  94.1 9.1 %copy.94 = f32[2,4,16384]{1,2,0:T(8,128)} copy(f32[2,4,16384]{2,1,0:T(4,128)} %param.30) | data formatting | bytes 1048576
  120.3 25.2 %all-gather.4 = f32[8,4,256]{2,1,0:T(4,128)S(1)} all-gather(f32[1,4,256]{2,1,0:T(4,128)S(1)} %maximum_bitcast_fusion.1), channel_id=3, replica_groups=mesh['sp_0'=8,'sp_1'=8,'sp_2'=2,'tp'=4] {'sp_1'}, dimensions={0}, use_global_device_ids=true | all-gather | bytes 36864 | tf_op jit(solution)/shard_map/all_gather | solution.py:46
  145.5 25.6 %all-gather.5 = f32[8,4,256]{2,1,0:T(4,128)S(1)} all-gather(f32[1,4,256]{2,1,0:T(4,128)S(1)} %maximum_bitcast_fusion.2), channel_id=4, replica_groups=mesh['sp_0'=8,'sp_1'=8,'sp_2'=2,'tp'=4] {'sp_0'}, dimensions={0}, use_global_device_ids=true | all-gather | bytes 36864 | tf_op jit(solution)/shard_map/all_gather | solution.py:46
  175.3 9.4 %all-gather.11.cloned.1.call-done = bf16[2,16384,128]{1,2,0:T(8,128)(2,1)} async-done(((bf16[2,128,128]{1,2,0:T(8,128)(2,1)}), bf16[2,16384,128]{1,2,0:T(8,128)(2,1)}) %all-gather.11.cloned.1.call-update) | async-done | bytes 8388624 | tf_op jit(solution)/shard_map/all_gather | solution.py:171
  184.7 332.4 %while.20 = (s32[]{:T(128)}, f32[2,1,512]{2,0,1:T(2,128)S(1)}, f32[2,1,512]{2,0,1:T(2,128)S(1)}, f32[2,1,512,64]{2,3,0,1:T(8,128)S(1)}, s32[]{:T(128)}, /*index=...) while((s32[]{:T(128)}, f32[2,1,512]{2,0,1:T(2,128)S(1)}, ...), condition=%wide.region_8.9_spmd.clone, body=%wide.region_3.8_spmd.clone.sunk | while | flops 278538752 | bytes 48562600 | solution.py:221
  184.8 20.7 %conditional.3 = ((f32[2,1,512]{2,0,1:T(2,128)S(1)}, f32[2,1,512]{2,0,1:T(2,128)S(1)}, f32[2,1,512,64]{2,3,0,1:T(8,128)S(1)})) conditional(s32[]{:T(128)} %convert_element_type.195, (f32[2,1,512]{2,0,1:T(2,128)S(1)}, f32[2,1,512]{2,0,1:T(2,128)S(1)}, f32[2,1,512,64]{2,3,0,1:T(8,128)S(1)}) %tuple.87, (s32[512]{0:T(512)S(1)}, s32[]{:T(128)}, s32[]{:T(128)}, ...), branch_computations={%region_4.0_spmd, %region_5.7_spmd} | conditional | flops 278538240 | bytes 48560300 | solution.py:217
  190.0 5.5 %sub.34 = f32[2,512,1024]{1,2,0:T(8,128)} reshape(f32[2,4,128,1024]{2,1,3,0:T(4,128)} %sub.33) | data formatting | bytes 8388608 | tf_op jit(solution)/shard_map/while/body/eval_jaxpr/cond/branch_1_fun/sub | solution.py:195
  205.5 20.7 %conditional.3 = ((f32[2,1,512]{2,0,1:T(2,128)S(1)}, f32[2,1,512]{2,0,1:T(2,128)S(1)}, f32[2,1,512,64]{2,3,0,1:T(8,128)S(1)})) conditional(s32[]{:T(128)} %convert_element_type.195, (f32[2,1,512]{2,0,1:T(2,128)S(1)}, f32[2,1,512]{2,0,1:T(2,128)S(1)}, f32[2,1,512,64]{2,3,0,1:T(8,128)S(1)}) %tuple.87, (s32[512]{0:T(512)S(1)}, s32[]{:T(128)}, s32[]{:T(128)}, ...), branch_computations={%region_4.0_spmd, %region_5.7_spmd} | conditional | flops 278538240 | bytes 48560300 | solution.py:217
  210.8 5.5 %sub.34 = f32[2,512,1024]{1,2,0:T(8,128)} reshape(f32[2,4,128,1024]{2,1,3,0:T(4,128)} %sub.33) | data formatting | bytes 8388608 | tf_op jit(solution)/shard_map/while/body/eval_jaxpr/cond/branch_1_fun/sub | solution.py:195
  226.3 20.7 %conditional.3 = ((f32[2,1,512]{2,0,1:T(2,128)S(1)}, f32[2,1,512]{2,0,1:T(2,128)S(1)}, f32[2,1,512,64]{2,3,0,1:T(8,128)S(1)})) conditional(s32[]{:T(128)} %convert_element_type.195, (f32[2,1,512]{2,0,1:T(2,128)S(1)}, f32[2,1,512]{2,0,1:T(2,128)S(1)}, f32[2,1,512,64]{2,3,0,1:T(8,128)S(1)}) %tuple.87, (s32[512]{0:T(512)S(1)}, s32[]{:T(128)}, s32[]{:T(128)}, ...), branch_computations={%region_4.0_spmd, %region_5.7_spmd} | conditional | flops 278538240 | bytes 48560300 | solution.py:217
  231.5 5.5 %sub.34 = f32[2,512,1024]{1,2,0:T(8,128)} reshape(f32[2,4,128,1024]{2,1,3,0:T(4,128)} %sub.33) | data formatting | bytes 8388608 | tf_op jit(solution)/shard_map/while/body/eval_jaxpr/cond/branch_1_fun/sub | solution.py:195
  247.1 20.7 %conditional.3 = ((f32[2,1,512]{2,0,1:T(2,128)S(1)}, f32[2,1,512]{2,0,1:T(2,128)S(1)}, f32[2,1,512,64]{2,3,0,1:T(8,128)S(1)})) conditional(s32[]{:T(128)} %convert_element_type.195, (f32[2,1,512]{2,0,1:T(2,128)S(1)}, f32[2,1,512]{2,0,1:T(2,128)S(1)}, f32[2,1,512,64]{2,3,0,1:T(8,128)S(1)}) %tuple.87, (s32[512]{0:T(512)S(1)}, s32[]{:T(128)}, s32[]{:T(128)}, ...), branch_computations={%region_4.0_spmd, %region_5.7_spmd} | conditional | flops 278538240 | bytes 48560300 | solution.py:217
  252.3 5.5 %sub.34 = f32[2,512,1024]{1,2,0:T(8,128)} reshape(f32[2,4,128,1024]{2,1,3,0:T(4,128)} %sub.33) | data formatting | bytes 8388608 | tf_op jit(solution)/shard_map/while/body/eval_jaxpr/cond/branch_1_fun/sub | solution.py:195
  267.9 20.7 %conditional.3 = ((f32[2,1,512]{2,0,1:T(2,128)S(1)}, f32[2,1,512]{2,0,1:T(2,128)S(1)}, f32[2,1,512,64]{2,3,0,1:T(8,128)S(1)})) conditional(s32[]{:T(128)} %convert_element_type.195, (f32[2,1,512]{2,0,1:T(2,128)S(1)}, f32[2,1,512]{2,0,1:T(2,128)S(1)}, f32[2,1,512,64]{2,3,0,1:T(8,128)S(1)}) %tuple.87, (s32[512]{0:T(512)S(1)}, s32[]{:T(128)}, s32[]{:T(128)}, ...), branch_computations={%region_4.0_spmd, %region_5.7_spmd} | conditional | flops 278538240 | bytes 48560300 | solution.py:217
  273.1 5.5 %sub.34 = f32[2,512,1024]{1,2,0:T(8,128)} reshape(f32[2,4,128,1024]{2,1,3,0:T(4,128)} %sub.33) | data formatting | bytes 8388608 | tf_op jit(solution)/shard_map/while/body/eval_jaxpr/cond/branch_1_fun/sub | solution.py:195
  288.6 20.7 %conditional.3 = ((f32[2,1,512]{2,0,1:T(2,128)S(1)}, f32[2,1,512]{2,0,1:T(2,128)S(1)}, f32[2,1,512,64]{2,3,0,1:T(8,128)S(1)})) conditional(s32[]{:T(128)} %convert_element_type.195, (f32[2,1,512]{2,0,1:T(2,128)S(1)}, f32[2,1,512]{2,0,1:T(2,128)S(1)}, f32[2,1,512,64]{2,3,0,1:T(8,128)S(1)}) %tuple.87, (s32[512]{0:T(512)S(1)}, s32[]{:T(128)}, s32[]{:T(128)}, ...), branch_computations={%region_4.0_spmd, %region_5.7_spmd} | conditional | flops 278538240 | bytes 48560300 | solution.py:217
  293.9 5.5 %sub.34 = f32[2,512,1024]{1,2,0:T(8,128)} reshape(f32[2,4,128,1024]{2,1,3,0:T(4,128)} %sub.33) | data formatting | bytes 8388608 | tf_op jit(solution)/shard_map/while/body/eval_jaxpr/cond/branch_1_fun/sub | solution.py:195
  309.4 20.7 %conditional.3 = ((f32[2,1,512]{2,0,1:T(2,128)S(1)}, f32[2,1,512]{2,0,1:T(2,128)S(1)}, f32[2,1,512,64]{2,3,0,1:T(8,128)S(1)})) conditional(s32[]{:T(128)} %convert_element_type.195, (f32[2,1,512]{2,0,1:T(2,128)S(1)}, f32[2,1,512]{2,0,1:T(2,128)S(1)}, f32[2,1,512,64]{2,3,0,1:T(8,128)S(1)}) %tuple.87, (s32[512]{0:T(512)S(1)}, s32[]{:T(128)}, s32[]{:T(128)}, ...), branch_computations={%region_4.0_spmd, %region_5.7_spmd} | conditional | flops 278538240 | bytes 48560300 | solution.py:217
  330.2 20.7 %conditional.3 = ((f32[2,1,512]{2,0,1:T(2,128)S(1)}, f32[2,1,512]{2,0,1:T(2,128)S(1)}, f32[2,1,512,64]{2,3,0,1:T(8,128)S(1)})) conditional(s32[]{:T(128)} %convert_element_type.195, (f32[2,1,512]{2,0,1:T(2,128)S(1)}, f32[2,1,512]{2,0,1:T(2,128)S(1)}, f32[2,1,512,64]{2,3,0,1:T(8,128)S(1)}) %tuple.87, (s32[512]{0:T(512)S(1)}, s32[]{:T(128)}, s32[]{:T(128)}, ...), branch_computations={%region_4.0_spmd, %region_5.7_spmd} | conditional | flops 278538240 | bytes 48560300 | solution.py:217
  351.0 20.7 %conditional.3 = ((f32[2,1,512]{2,0,1:T(2,128)S(1)}, f32[2,1,512]{2,0,1:T(2,128)S(1)}, f32[2,1,512,64]{2,3,0,1:T(8,128)S(1)})) conditional(s32[]{:T(128)} %convert_element_type.195, (f32[2,1,512]{2,0,1:T(2,128)S(1)}, f32[2,1,512]{2,0,1:T(2,128)S(1)}, f32[2,1,512,64]{2,3,0,1:T(8,128)S(1)}) %tuple.87, (s32[512]{0:T(512)S(1)}, s32[]{:T(128)}, s32[]{:T(128)}, ...), branch_computations={%region_4.0_spmd, %region_5.7_spmd} | conditional | flops 278538240 | bytes 48560300 | solution.py:217
  371.7 20.7 %conditional.3 = ((f32[2,1,512]{2,0,1:T(2,128)S(1)}, f32[2,1,512]{2,0,1:T(2,128)S(1)}, f32[2,1,512,64]{2,3,0,1:T(8,128)S(1)})) conditional(s32[]{:T(128)} %convert_element_type.195, (f32[2,1,512]{2,0,1:T(2,128)S(1)}, f32[2,1,512]{2,0,1:T(2,128)S(1)}, f32[2,1,512,64]{2,3,0,1:T(8,128)S(1)}) %tuple.87, (s32[512]{0:T(512)S(1)}, s32[]{:T(128)}, s32[]{:T(128)}, ...), branch_computations={%region_4.0_spmd, %region_5.7_spmd} | conditional | flops 278538240 | bytes 48560300 | solution.py:217
  377.0 5.5 %sub.34 = f32[2,512,1024]{1,2,0:T(8,128)} reshape(f32[2,4,128,1024]{2,1,3,0:T(4,128)} %sub.33) | data formatting | bytes 8388608 | tf_op jit(solution)/shard_map/while/body/eval_jaxpr/cond/branch_1_fun/sub | solution.py:195
  392.5 20.7 %conditional.3 = ((f32[2,1,512]{2,0,1:T(2,128)S(1)}, f32[2,1,512]{2,0,1:T(2,128)S(1)}, f32[2,1,512,64]{2,3,0,1:T(8,128)S(1)})) conditional(s32[]{:T(128)} %convert_element_type.195, (f32[2,1,512]{2,0,1:T(2,128)S(1)}, f32[2,1,512]{2,0,1:T(2,128)S(1)}, f32[2,1,512,64]{2,3,0,1:T(8,128)S(1)}) %tuple.87, (s32[512]{0:T(512)S(1)}, s32[]{:T(128)}, s32[]{:T(128)}, ...), branch_computations={%region_4.0_spmd, %region_5.7_spmd} | conditional | flops 278538240 | bytes 48560300 | solution.py:217
  397.7 5.5 %sub.34 = f32[2,512,1024]{1,2,0:T(8,128)} reshape(f32[2,4,128,1024]{2,1,3,0:T(4,128)} %sub.33) | data formatting | bytes 8388608 | tf_op jit(solution)/shard_map/while/body/eval_jaxpr/cond/branch_1_fun/sub | solution.py:195
  413.3 20.7 %conditional.3 = ((f32[2,1,512]{2,0,1:T(2,128)S(1)}, f32[2,1,512]{2,0,1:T(2,128)S(1)}, f32[2,1,512,64]{2,3,0,1:T(8,128)S(1)})) conditional(s32[]{:T(128)} %convert_element_type.195, (f32[2,1,512]{2,0,1:T(2,128)S(1)}, f32[2,1,512]{2,0,1:T(2,128)S(1)}, f32[2,1,512,64]{2,3,0,1:T(8,128)S(1)}) %tuple.87, (s32[512]{0:T(512)S(1)}, s32[]{:T(128)}, s32[]{:T(128)}, ...), branch_computations={%region_4.0_spmd, %region_5.7_spmd} | conditional | flops 278538240 | bytes 48560300 | solution.py:217
  434.1 20.7 %conditional.3 = ((f32[2,1,512]{2,0,1:T(2,128)S(1)}, f32[2,1,512]{2,0,1:T(2,128)S(1)}, f32[2,1,512,64]{2,3,0,1:T(8,128)S(1)})) conditional(s32[]{:T(128)} %convert_element_type.195, (f32[2,1,512]{2,0,1:T(2,128)S(1)}, f32[2,1,512]{2,0,1:T(2,128)S(1)}, f32[2,1,512,64]{2,3,0,1:T(8,128)S(1)}) %tuple.87, (s32[512]{0:T(512)S(1)}, s32[]{:T(128)}, s32[]{:T(128)}, ...), branch_computations={%region_4.0_spmd, %region_5.7_spmd} | conditional | flops 278538240 | bytes 48560300 | solution.py:217
  454.8 20.7 %conditional.3 = ((f32[2,1,512]{2,0,1:T(2,128)S(1)}, f32[2,1,512]{2,0,1:T(2,128)S(1)}, f32[2,1,512,64]{2,3,0,1:T(8,128)S(1)})) conditional(s32[]{:T(128)} %convert_element_type.195, (f32[2,1,512]{2,0,1:T(2,128)S(1)}, f32[2,1,512]{2,0,1:T(2,128)S(1)}, f32[2,1,512,64]{2,3,0,1:T(8,128)S(1)}) %tuple.87, (s32[512]{0:T(512)S(1)}, s32[]{:T(128)}, s32[]{:T(128)}, ...), branch_computations={%region_4.0_spmd, %region_5.7_spmd} | conditional | flops 278538240 | bytes 48560300 | solution.py:217
  475.6 20.7 %conditional.3 = ((f32[2,1,512]{2,0,1:T(2,128)S(1)}, f32[2,1,512]{2,0,1:T(2,128)S(1)}, f32[2,1,512,64]{2,3,0,1:T(8,128)S(1)})) conditional(s32[]{:T(128)} %convert_element_type.195, (f32[2,1,512]{2,0,1:T(2,128)S(1)}, f32[2,1,512]{2,0,1:T(2,128)S(1)}, f32[2,1,512,64]{2,3,0,1:T(8,128)S(1)}) %tuple.87, (s32[512]{0:T(512)S(1)}, s32[]{:T(128)}, s32[]{:T(128)}, ...), branch_computations={%region_4.0_spmd, %region_5.7_spmd} | conditional | flops 278538240 | bytes 48560300 | solution.py:217
  496.4 20.7 %conditional.3 = ((f32[2,1,512]{2,0,1:T(2,128)S(1)}, f32[2,1,512]{2,0,1:T(2,128)S(1)}, f32[2,1,512,64]{2,3,0,1:T(8,128)S(1)})) conditional(s32[]{:T(128)} %convert_element_type.195, (f32[2,1,512]{2,0,1:T(2,128)S(1)}, f32[2,1,512]{2,0,1:T(2,128)S(1)}, f32[2,1,512,64]{2,3,0,1:T(8,128)S(1)}) %tuple.87, (s32[512]{0:T(512)S(1)}, s32[]{:T(128)}, s32[]{:T(128)}, ...), branch_computations={%region_4.0_spmd, %region_5.7_spmd} | conditional | flops 278538240 | bytes 48560300 | solution.py:217
  501.6 5.5 %sub.34 = f32[2,512,1024]{1,2,0:T(8,128)} reshape(f32[2,4,128,1024]{2,1,3,0:T(4,128)} %sub.33) | data formatting | bytes 8388608 | tf_op jit(solution)/shard_map/while/body/eval_jaxpr/cond/branch_1_fun/sub | solution.py:195
  518.9 19.6 %all_to_all.5 = bf16[4,256,512]{2,1,0:T(8,128)(2,1)S(1)} all-to-all(bf16[4,256,512]{2,1,0:T(8,128)(2,1)S(1)} %bitcast.376), channel_id=1, replica_groups=mesh['sp_0'=8,'sp_1'=8,'sp_2'=2,'tp'=4] {'tp'}, dimensions={0} | all-to-all | bytes 2097152 | tf_op jit(solution)/shard_map/all_to_all | solution.py:78
  (452 shorter events, 312.6 us)
Async XLA Ops:
  6.5 511.3 %copy-start = (bf16[256,2048]{1,0:T(8,128)(2,1)S(1)}, bf16[256,2048]{1,0:T(8,128)(2,1)}, u32[]{:S(2)}) copy-start(bf16[256,2048]{1,0:T(8,128)(2,1)} %param.40) | copy-start | bytes 3145732
  6.5 86.8 %copy-start.12 = (f32[64]{0:T(128)S(1)}, f32[64]{0:T(128)}, u32[]{:S(2)}) copy-start(f32[64]{0:T(128)} %param.29) | copy-start | bytes 772
  6.5 83.5 %all-gather.9.cloned.1.call-start = ((), (), s32[]{:S(2)}) async-start(), calls=%async_computation.1 | async-start | bytes 3698688 | tf_op jit(solution)/shard_map/all_gather | solution.py:19
  8.1 176.6 %all-gather.11.cloned.1.call-start = ((), (), s32[]{:S(2)}) async-start(), calls=%async_computation.2 | async-start | bytes 8454144 | tf_op jit(solution)/shard_map/all_gather | solution.py:171
  94.1 9.9 %copy-start.11 = (f32[256]{0:T(256)S(1)}, f32[256]{0:T(256)}, u32[]{:S(2)}) copy-start(f32[256]{0:T(256)} %param.36) | copy-start | bytes 3076
  94.1 9.9 %copy-start.8 = (bf16[4,256]{1,0:T(4,128)(2,1)S(1)}, bf16[4,256]{1,0:T(4,128)(2,1)}, u32[]{:S(2)}) copy-start(bf16[4,256]{1,0:T(4,128)(2,1)} %param.33) | copy-start | bytes 6148
  94.1 9.9 %copy-start.2 = (bf16[2,128,2048]{2,1,0:T(8,128)(2,1)S(1)}, bf16[2,128,2048]{2,1,0:T(8,128)(2,1)}, u32[]{:S(2)}) copy-start(bf16[2,128,2048]{2,1,0:T(8,128)(2,1)} %param.23) | copy-start | bytes 3145732
  94.1 9.9 %copy-start.7 = (f32[2048]{0:T(1024)S(1)}, f32[2048]{0:T(1024)}, u32[]{:S(2)}) copy-start(f32[2048]{0:T(1024)} %param.24) | copy-start | bytes 24580
  105.4 6.7 %copy-start.3 = (bf16[2,128,2048]{2,1,0:T(8,128)(2,1)S(1)}, bf16[2,128,2048]{2,1,0:T(8,128)(2,1)}, u32[]{:S(2)}) copy-start(bf16[2,128,2048]{2,1,0:T(8,128)(2,1)} %multiply_convert_fusion) | copy-start | bytes 3145732
  107.2 6.7 %copy-start.13 = (f32[64]{0:T(128)S(1)}, f32[64]{0:T(128)}, u32[]{:S(2)}) copy-start(f32[64]{0:T(128)} %param.28) | copy-start | bytes 772
  107.2 7.0 %collective-permute-start = (bf16[2,3,256]{2,1,0:T(4,128)(2,1)S(1)}, bf16[2,3,256]{2,1,0:T(4,128)(2,1)S(1)}, u32[]{:S(2)}, u32[]{:S(2)}) collective-permute-start(bf16[2,3,256]{2,1,0:T(4,128)(2,1)S(1)} %slice.520), channel_id=1, source_target_pairs={{0,4},{4,8},{8,12},{12,16},{16,20},{20,24},{24,28},{28,32},{32,36}... | collective-permute-start | bytes 9224 | tf_op jit(solution)/shard_map/ppermute | solution.py:29
  110.6 3.8 copy-start.14
  112.1 2.8 copy-start.15
  117.3 53.9 %copy-start.4 = (bf16[2,128,2048]{2,1,0:T(8,128)(2,1)S(1)}, bf16[2,128,2048]{2,1,0:T(8,128)(2,1)}, u32[]{:S(2)}) copy-start(bf16[2,128,2048]{2,1,0:T(8,128)(2,1)} %multiply_convert_fusion) | copy-start | bytes 3145732
  118.1 57.0 %copy-start.9 = (f32[256]{0:T(256)S(1)}, f32[256]{0:T(256)}, u32[]{:S(2)}) copy-start(f32[256]{0:T(256)} %param.39) | copy-start | bytes 3076
  184.7 333.0 %copy-start.10 = (f32[256]{0:T(256)S(1)}, f32[256]{0:T(256)}, u32[]{:S(2)}) copy-start(f32[256]{0:T(256)} %param.38) | copy-start | bytes 3076
  201.4 3.5 copy-start.1
  222.1 3.5 copy-start.1
  242.9 3.5 copy-start.1
  263.7 3.5 copy-start.1
  284.5 3.5 copy-start.1
  305.2 3.5 copy-start.1
  326.0 3.5 copy-start.1
  346.8 3.5 copy-start.1
  367.6 3.5 copy-start.1
  388.3 3.5 copy-start.1
  409.1 3.5 copy-start.1
  429.9 3.5 copy-start.1
  450.7 3.5 copy-start.1
  471.4 3.5 copy-start.1
  492.2 3.5 copy-start.1
  513.0 3.5 copy-start.1
  (2 other events, 2.7 us)
Sparse Core Ops, SparseCore 0:
  10.5 79.5 all-gather.8
  94.2 90.4 all-gather.10
where the time goes:
time: 549 us; the launch traced here: 546 us
  local copies, waits for them, and re-layouts  194 us (35%)
  matrix products  150 us (27%)
  waiting for transfers between devices  88.3 us (16%)
  blocking collectives  72.2 us (13%)
  other arithmetic  23.2 us (4%)
  between operations  14.6 us (3%)
    sub x32, local copies, waits for them, and re-layouts, work(): scores.reshape(seq_count, kv_local, head_group, seq_span, sub_size)  150 us
    dot_general x16, matrix products, work(): jnp.einsum('bhqd,bkhd->bhqk', queries, key_block, preferred_element_type=...  87.4 us
    all_gather x1, waiting for transfers between devices, side_by_side(): lax.all_gather(both, axis, axis=dim, tiled=True)  78.8 us
    all_gather x3, blocking collectives, collected_together(): both, at, found = (lax.all_gather(jnp.concatenate(lines), axis), 0, {})  52.6 us
    dot_general x16, matrix products, work(): jnp.einsum('bhqk,bkhd->bhqd', weights.astype(jnp.bfloat16), value_block,...  51.7 us
    dynamic_slice x16, local copies, waits for them, and re-layouts, work(): key_gates = lax.dynamic_slice_in_dim(forget_cache, key_first, sub_size, 2)  20.8 us
    all_to_all x1, blocking collectives, sent_and_summed(): parts = lax.all_to_all(in_blocks(shard, dim, peers), axis, 0, 0, tiled=True)  19.6 us
  transfers between devices with their start and end apart: 3, of which 2 were waited for; matrix products, arithmetic and copies ran while one was open for 5% of the time, Pallas kernels for 0%

commit v1 on v0

--- a/solution.py
+++ b/solution.py
@@ -1,6 +1,10 @@
+import functools
+
 import jax
 import jax.numpy as jnp
 from jax import lax
+from jax.experimental import pallas as pl
+from jax.experimental.pallas import tpu as pltpu
 from jax.sharding import Mesh
 from jax.sharding import PartitionSpec as P
 
@@ -88,16 +92,87 @@
     return (earlier[0] * later[0], later[0] * earlier[1] + later[1])
 
 
-def block_length(length, span):
-    shards = max(length // span, 1)
-    group_size = 1
-    for trial_size in range(1, shards + 1):
-        if shards % trial_size == 0 and trial_size * span <= 1024:
-            group_size = trial_size
-    sub_size = group_size * span
-    if length % sub_size:
-        sub_size = length
-    return sub_size
+NT = (((1,), (1,)), ((), ()))
+
+def gate_pieces(rel):
+    hi = rel.astype(jnp.bfloat16)
+    rest = rel - hi.astype(jnp.float32)
+    mid = rest.astype(jnp.bfloat16)
+    low = (rest - mid.astype(jnp.float32)).astype(jnp.bfloat16)
+    f = jnp.float32
+    return jnp.concatenate([hi.astype(f), mid.astype(f), low.astype(f), jnp.zeros_like(rel)], axis=0).astype(jnp.bfloat16)
+
+def attn_kernel(place, CB, q_ref, own_ref, kv_ref, forget_ref, gain_ref, out_ref, gates, acc, top):
+    seqs, rows, depth = q_ref.shape
+    span = own_ref.shape[2]
+    me = place()
+    first = pl.multiple_of(me * span, span)
+    length = forget_ref.shape[2]
+    chunk = CB * span
+    ones_own = jnp.ones((16, span), jnp.bfloat16)
+    ones = jnp.ones((16, chunk), jnp.bfloat16)
+    step = 2048 if length % 2048 == 0 else length
+    row = lax.broadcasted_iota(jnp.int32, (rows, span), 0) % span
+    col = lax.broadcasted_iota(jnp.int32, (rows, span), 1)
+    count = (me + CB - 1) // CB
+    for b in range(seqs):
+        base = forget_ref[b, :, pl.ds(first, span)][:, :1]
+        rel_own = base - forget_ref[b, :, pl.ds(first, span)]
+        def prep(c, _):
+            at = pl.multiple_of(c * chunk, chunk)
+            rel = base - forget_ref[b, :, pl.ds(at, chunk)]
+            pos = at + lax.broadcasted_iota(jnp.int32, rel.shape, 1)
+            rel = jnp.where(pos < first, rel, -1e30)
+            gates[b, :, pl.ds(at, chunk)] = gate_pieces(rel)
+            return 0
+        lax.fori_loop(0, count, prep, 0)
+        own = own_ref[b]
+        rhs = jnp.concatenate([own[:64], gate_pieces(rel_own)], axis=0)
+        s = jnp.dot(q_ref[b], rhs, preferred_element_type=jnp.float32)
+        s = jnp.where(row >= col, s, -jnp.inf)
+        m = jnp.max(s, axis=1, keepdims=True)
+        p = jnp.exp(s - m).astype(jnp.bfloat16)
+        acc[b] = lax.dot_general(p, jnp.concatenate([own[64:], ones_own], axis=0), NT, preferred_element_type=jnp.float32)
+        top[b] = jnp.broadcast_to(m, (rows, 128))
+
+    def work(c, _):
+        at = pl.multiple_of(c * chunk, chunk)
+        for b in range(seqs):
+            blocks = [kv_ref[c * CB + i, b] for i in range(CB)]
+            kt = jnp.concatenate([x[:64] for x in blocks], axis=1)
+            vt = jnp.concatenate([x[64:] for x in blocks], axis=1)
+            rhs = jnp.concatenate([kt, gates[b, :, pl.ds(at, chunk)]], axis=0)
+            vx = jnp.concatenate([vt, ones], axis=0)
+            s = jnp.dot(q_ref[b], rhs, preferred_element_type=jnp.float32)
+            old = top[b][:, :1]
+            m = jnp.maximum(old, jnp.max(s, axis=1, keepdims=True))
+            p = jnp.exp(s - m).astype(jnp.bfloat16)
+            fade = jnp.exp(old - m)
+            acc[b] = acc[b] * fade + lax.dot_general(p, vx, NT, preferred_element_type=jnp.float32)
+            top[b] = jnp.broadcast_to(m, (rows, 128))
+        return 0
+    lax.fori_loop(0, count, work, 0)
+    heads = rows // span
+    for b in range(seqs):
+        a = acc[b]
+        att = a[:, :64] / a[:, 64:65]
+        att = att * lax.rsqrt(jnp.mean(att * att, axis=1, keepdims=True) + 1e-6)
+        wide = jnp.concatenate([att[h * span:(h + 1) * span] for h in range(heads)], axis=1)
+        out_ref[b] = (wide * gain_ref[...]).astype(jnp.bfloat16)
+
+def attention(place, q, own, kv, forget, gain, CB=8):
+    seqs, rows, depth = q.shape
+    span = own.shape[2]
+    length = forget.shape[2]
+    heads = rows // span
+    return pl.pallas_call(
+        functools.partial(attn_kernel, place, CB),
+        out_shape=jax.ShapeDtypeStruct((seqs, span, heads * 64), jnp.bfloat16),
+        in_specs=[pl.BlockSpec(memory_space=pltpu.VMEM)] * 5,
+        out_specs=pl.BlockSpec(memory_space=pltpu.VMEM),
+        scratch_shapes=[pltpu.VMEM((seqs, 16, length), jnp.bfloat16), pltpu.VMEM((seqs, rows, 80), jnp.float32), pltpu.VMEM((seqs, rows, 128), jnp.float32)],
+        compiler_params=pltpu.CompilerParams(vmem_limit_bytes=60 * 1024 * 1024),
+    )(q, own, kv, forget, gain)
 
 
 def body(
@@ -126,7 +201,6 @@
     head_dim = query_gain.shape[0]
     att_local = query_weight.shape[1] // head_dim
     kv_local = key_weight.shape[1] // head_dim
-    head_group = att_local // kv_local
     channels = rec_in_weight.shape[1]
     normed = rms_scale(
         inputs.reshape(row_count, model_width).astype(jnp.float32), norm_gain
@@ -148,83 +222,20 @@
     queries = rms_scale(query_proj.reshape(row_count, att_local, head_dim), query_gain).astype(
         jnp.bfloat16
     )
-    queries = queries.reshape(seq_count, seq_span, kv_local, head_group, head_dim).transpose(
-        0, 2, 3, 1, 4
-    )
-    queries = queries.reshape(seq_count, kv_local, head_group * seq_span, head_dim)
+    queries = (queries * jnp.bfloat16(head_dim ** (-0.5))).reshape(seq_count, seq_span, att_local, head_dim)
+    queries = queries.transpose(0, 2, 1, 3)
+    picks = jnp.tile(jnp.eye(att_local, dtype=jnp.bfloat16), (1, 4)) * (jnp.arange(16) < 12).astype(jnp.bfloat16)
+    picks = jnp.broadcast_to(picks[None, :, None, :], (seq_count, att_local, seq_span, 16))
+    queries = jnp.concatenate([queries, picks], axis=3).reshape(seq_count, att_local * seq_span, head_dim + 16)
     key_heads = rms_scale(key_proj.reshape(row_count, kv_local, head_dim), key_gain).astype(
         jnp.bfloat16
     )
     key_heads = key_heads.reshape(seq_count, seq_span, kv_cols)
     value_heads = value_sum.astype(jnp.bfloat16).reshape(seq_count, seq_span, kv_cols)
-    key_value = jnp.concatenate([key_heads, value_heads], axis=2)
-    my_first = lax.axis_index(SP) * seq_span
-    own_gates = lax.dynamic_slice_in_dim(forget_cache, my_first, seq_span, 2)
-    own_gates = own_gates.reshape(seq_count, kv_local, head_group, seq_span, 1)
-    query_pos = my_first + jnp.tile(jnp.arange(seq_span, dtype=jnp.int32), head_group)
-    scaling = head_dim ** (-0.5)
-    start_state = (
-        jnp.full((seq_count, kv_local, head_group * seq_span), -jnp.inf, jnp.float32),
-        jnp.zeros((seq_count, kv_local, head_group * seq_span), jnp.float32),
-        jnp.zeros((seq_count, kv_local, head_group * seq_span, head_dim), jnp.float32),
-    )
-    shard_part = lax.all_gather(key_value, SP, axis=1, tiled=True)
-    offset = jnp.int32(0)
-    length = shard_part.shape[1]
-    sub_size = block_length(length, seq_span)
-
-    def one_step(block_index, carried_state):
-        key_first = offset + block_index * sub_size
-
-        def work(carried):
-            top_score, totals, accum = carried
-            block_rows = lax.dynamic_slice_in_dim(shard_part, block_index * sub_size, sub_size, 1)
-            key_block = block_rows[:, :, :kv_cols].reshape(seq_count, sub_size, kv_local, head_dim)
-            value_block = block_rows[:, :, kv_cols:].reshape(
-                seq_count, sub_size, kv_local, head_dim
-            )
-            key_gates = lax.dynamic_slice_in_dim(forget_cache, key_first, sub_size, 2)
-            key_gates = key_gates.reshape(seq_count, kv_local, head_group, 1, sub_size)
-            scores = (
-                jnp.einsum(
-                    "bhqd,bkhd->bhqk", queries, key_block, preferred_element_type=jnp.float32
-                )
-                * scaling
-            )
-            scores = (
-                scores.reshape(seq_count, kv_local, head_group, seq_span, sub_size)
-                + own_gates
-                - key_gates
-            )
-            scores = scores.reshape(seq_count, kv_local, head_group * seq_span, sub_size)
-            visible = (
-                query_pos[:, None] >= (key_first + jnp.arange(sub_size, dtype=jnp.int32))[None, :]
-            )
-            scores = jnp.where(visible, scores, -jnp.inf)
-            new_top = jnp.maximum(top_score, jnp.max(scores, axis=-1))
-            safe_top = jnp.where(jnp.isfinite(new_top), new_top, 0.0)
-            weights = jnp.exp(scores - safe_top[..., None])
-            fading = jnp.exp(top_score - safe_top)
-            totals = totals * fading + jnp.sum(weights, axis=-1)
-            accum = accum * fading[..., None] + jnp.einsum(
-                "bhqk,bkhd->bhqd",
-                weights.astype(jnp.bfloat16),
-                value_block,
-                preferred_element_type=jnp.float32,
-            )
-            return (new_top, totals, accum)
-
-        return lax.cond(
-            key_first < my_first + seq_span, work, lambda carried: carried, carried_state
-        )
-
-    top_score, totals, accum = lax.fori_loop(0, length // sub_size, one_step, start_state)
-    attended = (accum / totals[..., None]).reshape(
-        seq_count, kv_local, head_group, seq_span, head_dim
-    )
-    attended = attended.transpose(0, 3, 1, 2, 4).reshape(row_count, att_local, head_dim)
-    att_normed = rms_scale(attended, attn_out_gain.reshape(att_local, head_dim)).astype(
-        jnp.bfloat16
+    key_value = jnp.concatenate([key_heads, value_heads], axis=2).transpose(0, 2, 1)
+    gathered = lax.all_gather(key_value, SP, axis=0)
+    att_normed = attention(
+        lambda: lax.axis_index(SP), queries, key_value, gathered, forget_cache, attn_out_gain[None], CB=32
     )
     att_normed = att_normed.reshape(row_count, att_local * head_dim)
     rec_in = rec_in_sum.astype(jnp.bfloat16).reshape(seq_count, seq_span, channels)

time: 549 us -> 241 us (0.44)
  the two profiles are of different devices: /device:TPU:504 before, /device:TPU:448 now
where the time goes in v1:
time: 241 us; the launch traced here: 240 us
  waiting for transfers between devices  93.2 us (39%)
  blocking collectives  71.3 us (30%)
  Pallas kernels  29.9 us (12%)
  between operations  14.4 us (6%)
  matrix products  12.4 us (5%)
  local copies, waits for them, and re-layouts  8.36 us (3%)
  other arithmetic  8.11 us (3%)
    all_gather x1, waiting for transfers between devices, side_by_side(): lax.all_gather(both, axis, axis=dim, tiled=True)  80.8 us
    all_gather x3, blocking collectives, collected_together(): both, at, found = (lax.all_gather(jnp.concatenate(lines), axis), 0, {})  51.8 us
    pallas_call x1, Pallas kernels, attention(): pl.pallas_call(functools.partial(attn_kernel, place, CB), out_shape=jax.S...  29.9 us
    all_to_all x1, blocking collectives, sent_and_summed(): parts = lax.all_to_all(in_blocks(shard, dim, peers), axis, 0, 0, tiled=True)  19.5 us
    all_gather x1, waiting for transfers between devices, body(): gathered = lax.all_gather(key_value, SP, axis=0)  12.4 us
    dot_general x5, matrix products, body(): lax.dot_general(normed_cols, weight_part, row_contract, preferred_element...  9.08 us
  transfers between devices with their start and end apart: 3, of which 2 were waited for; matrix products, arithmetic and copies ran while one was open for 9% of the time, Pallas kernels for 0%

profile of v1, /device:TPU:448, one launch (start us, length us, event | category | flops | bytes accessed | tf_op | source)
XLA Modules:
  0.0 240.0 jit_solution(5904879185916049885)
XLA Ops:
  6.5 1.5 concatenate.57
  8.2 1.5 multiply_reduce_fusion
  9.7 1.6 fusion.2
  11.3 80.8 %all-gather.10.cloned.1.call-done = bf16[2048,896]{1,0:T(8,128)(2,1)} async-done(((bf16[16,896]{1,0:T(8,128)(2,1)}), bf16[2048,896]{1,0:T(8,128)(2,1)}) %all-gather.10.cloned.1.call-update) | async-done | bytes 3670032 | tf_op jit(solution)/shard_map/all_gather | solution.py:23
  92.1 1.5 multiply_reduce_fusion.2
  93.6 1.7 fusion.11
  95.4 0.6 maximum_bitcast_fusion.own_ref
  96.2 1.3 multiply_convert_fusion
  97.6 1.7 convolution_convert_fusion
  99.3 2.3 collective-permute-start
  101.6 1.3 slice_bitcast_fusion.2
  102.8 1.4 copy.79
  104.3 1.7 multiply_reduce_fusion.1
  106.2 0.2 copy.80
  106.4 0.9 pad_maximum_fusion
  107.3 0.1 add_convert_fusion
  107.6 0.3 fusion.10
  107.9 0.1 copy.87
  108.0 1.1 fusion.6
  109.3 0.2 convert_multiply_fusion
  112.4 2.4 %all-gather.4 = f32[2,4,256]{2,1,0:T(4,128)S(1)} all-gather(f32[1,4,256]{2,1,0:T(4,128)S(1)} %maximum_bitcast_fusion.1), channel_id=3, replica_groups=mesh['sp_0'=8,'sp_1'=8,'sp_2'=2,'tp'=4] {'sp_2'}, dimensions={0}, use_global_device_ids=true | all-gather | bytes 12288 | tf_op jit(solution)/shard_map/all_gather | solution.py:50
  114.8 24.7 %all-gather.5 = f32[8,4,256]{2,1,0:T(4,128)S(1)} all-gather(f32[1,4,256]{2,1,0:T(4,128)S(1)} %maximum_bitcast_fusion.2), channel_id=4, replica_groups=mesh['sp_0'=8,'sp_1'=8,'sp_2'=2,'tp'=4] {'sp_1'}, dimensions={0}, use_global_device_ids=true | all-gather | bytes 36864 | tf_op jit(solution)/shard_map/all_gather | solution.py:50
  139.5 24.7 %all-gather.6 = f32[8,4,256]{2,1,0:T(4,128)S(1)} all-gather(f32[1,4,256]{2,1,0:T(4,128)S(1)} %maximum_bitcast_fusion.3), channel_id=5, replica_groups=mesh['sp_0'=8,'sp_1'=8,'sp_2'=2,'tp'=4] {'sp_0'}, dimensions={0}, use_global_device_ids=true | all-gather | bytes 36864 | tf_op jit(solution)/shard_map/all_gather | solution.py:50
  164.2 2.5 %fusion.74 = (f32[2,128,256]{2,1,0:T(8,128)}, f32[2,128,256]{2,1,0:T(8,128)S(1)}) fusion(bf16[2,128,2048]{2,1,0:T(8,128)(2,1)S(1)} %copy-done.2, bf16[2048,896]{1,0:T(8,128)(2,1)} %all-gather.10.cloned.1.call-done, f32[2,256]{1,0:T(2,128)S(1)} %fusion.48, f32[2,128,256]{2,1,0:T(8,128)S(1)} %pad.112, f32[2,128,256]{2,1,0:T(8,128)S(1)} %pad.113, ...), kind=kOutput, calls=%fused_computation.190 | convolution fusion | flops 269352960 | bytes 3672064 | tf_op jit(solution)/shard_map/dot_general | solution.py:216
  166.8 1.1 copy.93
  167.9 0.2 mul.595
  168.4 12.4 %all-gather.12.cloned.1.call-done = bf16[256,128,128]{2,1,0:T(8,128)(2,1)} async-done(((bf16[2,128,128]{2,1,0:T(8,128)(2,1)}), bf16[256,128,128]{2,1,0:T(8,128)(2,1)}) %all-gather.12.cloned.1.call-update) | async-done | bytes 8388624 | tf_op jit(solution)/shard_map/all_gather | solution.py:236
  180.8 29.9 %shard_map.181 = bf16[2,128,256]{2,1,0:T(8,128)(2,1)} custom-call(bf16[2,512,80]{2,1,0:T(8,128)(2,1)} %bitcast.319, bf16[2,128,128]{2,1,0:T(8,128)(2,1)} %maximum_bitcast_fusion.own_ref, bf16[128,2,128,128]{3,2,1,0:T(8,128)(2,1)} %bitcast.315, f32[2,4,16384]{2,1,0:T(4,128)} %forget_ref.1, f32[1,256]{1,0:T(1,128)} %bitcast.347), custom_call_target="tpu_custom_call" | custom-call | tf_op jit(solution)/shard_map/pallas_call | solution.py:168
  210.7 1.4 fusion.75
  212.2 0.5 fusion
  212.7 19.5 %all_to_all.5 = bf16[4,256,512]{2,1,0:T(8,128)(2,1)S(1)} all-to-all(bf16[4,256,512]{2,1,0:T(8,128)(2,1)S(1)} %bitcast.317), channel_id=1, replica_groups=mesh['sp_0'=8,'sp_1'=8,'sp_2'=2,'tp'=4] {'tp'}, dimensions={0} | all-to-all | bytes 2097152 | tf_op jit(solution)/shard_map/all_to_all | solution.py:82
  232.3 0.9 reduce_sum.52
  (168 shorter events, 3.5 us)
Async XLA Ops:
  6.5 204.2 %copy-start = (bf16[256,2048]{1,0:T(8,128)(2,1)S(1)}, bf16[256,2048]{1,0:T(8,128)(2,1)}, u32[]{:S(2)}) copy-start(bf16[256,2048]{1,0:T(8,128)(2,1)} %param.36) | copy-start | bytes 3145732
  6.5 85.5 %all-gather.10.cloned.1.call-start = ((), (), s32[]{:S(2)}) async-start(), calls=%async_computation.1 | async-start | bytes 3698688 | tf_op jit(solution)/shard_map/all_gather | solution.py:23
  8.1 172.7 %all-gather.12.cloned.1.call-start = ((), (), s32[]{:S(2)}) async-start(), calls=%async_computation.2 | async-start | bytes 8454144 | tf_op jit(solution)/shard_map/all_gather | solution.py:236
  11.2 84.1 %copy-start.9 = (f32[64]{0:T(128)S(1)}, f32[64]{0:T(128)}, u32[]{:S(2)}) copy-start(f32[64]{0:T(128)} %param.25) | copy-start | bytes 772
  11.2 84.9 %copy-start.8 = (f32[256]{0:T(256)S(1)}, f32[256]{0:T(256)}, u32[]{:S(2)}) copy-start(f32[256]{0:T(256)} %param.32) | copy-start | bytes 3076
  11.3 85.0 %copy-start.6 = (bf16[4,256]{1,0:T(4,128)(2,1)S(1)}, bf16[4,256]{1,0:T(4,128)(2,1)}, u32[]{:S(2)}) copy-start(bf16[4,256]{1,0:T(4,128)(2,1)} %param.29) | copy-start | bytes 6148
  11.3 85.0 %copy-start.1 = (bf16[2,128,2048]{2,1,0:T(8,128)(2,1)S(1)}, bf16[2,128,2048]{2,1,0:T(8,128)(2,1)}, u32[]{:S(2)}) copy-start(bf16[2,128,2048]{2,1,0:T(8,128)(2,1)} %param.19) | copy-start | bytes 3145732
  11.3 85.0 %copy-start.5 = (f32[2048]{0:T(1024)S(1)}, f32[2048]{0:T(1024)}, u32[]{:S(2)}) copy-start(f32[2048]{0:T(1024)} %param.20) | copy-start | bytes 24580
  99.3 5.0 %copy-start.2 = (bf16[2,128,2048]{2,1,0:T(8,128)(2,1)S(1)}, bf16[2,128,2048]{2,1,0:T(8,128)(2,1)}, u32[]{:S(2)}) copy-start(bf16[2,128,2048]{2,1,0:T(8,128)(2,1)} %multiply_convert_fusion) | copy-start | bytes 3145732
  99.3 8.0 %collective-permute-start = (bf16[2,3,256]{2,1,0:T(4,128)(2,1)S(1)}, bf16[2,3,256]{2,1,0:T(4,128)(2,1)S(1)}, u32[]{:S(2)}, u32[]{:S(2)}) collective-permute-start(bf16[2,3,256]{2,1,0:T(4,128)(2,1)S(1)} %slice.514), channel_id=1, source_target_pairs={{0,4},{4,8},{8,12},{12,16},{16,20},{20,24},{24,28},{28,32},{32,36}... | collective-permute-start | bytes 9224 | tf_op jit(solution)/shard_map/ppermute | solution.py:33
  104.3 1.8 copy-start.10
  106.0 1.5 copy-start.11
  107.5 1.7 copy-start.4
  164.2 4.0 %copy-start.7 = (f32[256]{0:T(256)S(1)}, f32[256]{0:T(256)}, u32[]{:S(2)}) copy-start(f32[256]{0:T(256)} %param.35) | copy-start | bytes 3076
  210.7 1.4 copy-start.3
Sparse Core Ops, SparseCore 0:
  10.5 81.4 all-gather.9
  96.1 84.6 all-gather.11

commit v2 on v1

v2 whole, which is shorter than its diff:
```python
import functools

import jax
import jax.numpy as jnp
from jax import lax
from jax.experimental import pallas as pl
from jax.experimental.pallas import tpu as pltpu
from jax.sharding import Mesh
from jax.sharding import PartitionSpec as P

SP = ("sp_0", "sp_1", "sp_2")
NT = (((1,), (1,)), ((), ()))
EPS = 1e-6
HALO = 16
F32, BF16 = jnp.float32, jnp.bfloat16
VMEM = pl.BlockSpec(memory_space=pltpu.VMEM)

MESH = pl.DeviceIdType.MESH
RING = 8


class Torus:
    def __init__(self, streams, sems, subs):
        self.streams, self.subs = streams, subs
        self.s1, self.r1, self.s2, self.r2, self.ps, self.pr = sems
        self.z, self.y, self.c = (lax.axis_index(n) for n in ("sp_0", "sp_1", "sp_2"))
        self.sign = 1 - 2 * self.c
        self.other = {"sp_2": 1 - self.c}
        self.pending = []

    def signals(self):
        z, y = self.z, self.y
        return [
            {"sp_0": lax.rem(z + 1, RING)},
            {"sp_0": lax.rem(z + RING - 1, RING)},
            {"sp_1": lax.rem(y + 1, RING)},
            {"sp_1": lax.rem(y + RING - 1, RING)},
            self.other,
        ]

    def places(self, k):
        return (self.y, self.z) if self.streams[k][2] == "y" else (self.z, self.y)

    def one(self, k, i):
        o, first = self.streams[k][1:]
        return o.at[self.z, i, self.c] if first == "y" else o.at[i, self.y, self.c]

    def many(self, k, i0, n, j, core):
        o, first = self.streams[k][1:]
        return o.at[j, pl.ds(i0, n), core] if first == "y" else o.at[pl.ds(i0, n), j, core]

    def back(self, pos, d, s):
        sg = self.sign if d == 0 else -self.sign
        return lax.rem(pos - sg * s + RING, RING)

    def ahead(self, k, phase, d):
        name = self.streams[k][2]
        first, second = ("sp_1", "sp_0") if name == "y" else ("sp_0", "sp_1")
        pos = self.places(k)[phase]
        return {(first, second)[phase]: self.back(pos, d, -1)}

    def go(self, src, dst, send, recv, device):
        copy = pltpu.make_async_remote_copy(
            src_ref=src, dst_ref=dst, send_sem=send, recv_sem=recv, device_id=device, device_id_type=MESH
        )
        copy.start()
        self.pending.append(copy)

    def arrived(self, ref, send, recv):
        pltpu.make_async_remote_copy(
            src_ref=ref, dst_ref=ref, send_sem=send, recv_sem=recv, device_id=self.other, device_id_type=MESH
        ).wait_recv()

    def steps(self, d):
        return 4 if d == 0 else 3

    def send1(self, k, d, s):
        pos = self.places(k)[0]
        dst = self.one(k, self.back(pos, d, s - 1))
        self.go(self.streams[k][0] if s == 1 else dst, dst, self.s1.at[k, d, s - 1], self.r1.at[k, d, s - 1], self.ahead(k, 0, d))

    def span(self, k, u):
        n = RING // self.subs[k]
        return u * n, n

    def send2(self, k, d, s, u):
        j = self.back(self.places(k)[1], d, s - 1)
        ref = self.many(k, *self.span(k, u), j, self.c)
        self.go(ref, ref, self.s2.at[k, d, s - 1, u], self.r2.at[k, d, s - 1, u], self.ahead(k, 1, d))

    def begin(self):
        for k in range(len(self.streams)):
            for d in (0, 1):
                self.send1(k, d, 1)
        for k in range(len(self.streams)):
            self.streams[k][1][self.z, self.y, self.c] = self.streams[k][0][...]

    def finish(self):
        ks = range(len(self.streams))
        for s in range(1, 5):
            for k in ks:
                for d in (0, 1):
                    if s <= self.steps(d):
                        got = self.one(k, self.back(self.places(k)[0], d, s))
                        self.arrived(got, self.s1.at[k, d, s - 1], self.r1.at[k, d, s - 1])
                        if s < self.steps(d):
                            self.send1(k, d, s + 1)
        for k in ks:
            for u in range(self.subs[k]):
                for d in (0, 1):
                    self.send2(k, d, 1, u)
        for k in ks:
            ref = self.many(k, 0, RING, self.places(k)[1], self.c)
            self.go(ref, ref, self.ps.at[k, 0, 0, 0], self.pr.at[k, 0, 0, 0], self.other)
        for s in range(1, 5):
            for u in range(max(self.subs)):
                for k in ks:
                    if u >= self.subs[k]:
                        continue
                    for d in (0, 1):
                        if s <= self.steps(d):
                            j = self.back(self.places(k)[1], d, s)
                            got = self.many(k, *self.span(k, u), j, self.c)
                            self.arrived(got, self.s2.at[k, d, s - 1, u], self.r2.at[k, d, s - 1, u])
                            if s < self.steps(d):
                                self.send2(k, d, s + 1, u)
                            self.go(got, got, self.ps.at[k, d, s, u], self.pr.at[k, d, s, u], self.other)
        for k in ks:
            ref = self.many(k, 0, RING, self.places(k)[1], 1 - self.c)
            self.arrived(ref, self.ps.at[k, 0, 0, 0], self.pr.at[k, 0, 0, 0])
        for s in range(1, 5):
            for k in ks:
                for u in range(self.subs[k]):
                    for d in (0, 1):
                        if s <= self.steps(d):
                            j = self.back(self.places(k)[1], d, -s)
                            got = self.many(k, *self.span(k, u), j, 1 - self.c)
                            self.arrived(got, self.ps.at[k, d, s, u], self.pr.at[k, d, s, u])
        for copy in self.pending:
            copy.wait_send()


def torus_sems(n, sub):
    dma = pltpu.SemaphoreType.DMA
    return [dma((n, 2, 4)), dma((n, 2, 4)), dma((n, 2, 4, sub)), dma((n, 2, 4, sub)), dma((n, 2, 5, sub)), dma((n, 2, 5, sub))]


def meet(devices):
    barrier = pltpu.get_barrier_semaphore()
    for device in devices:
        pl.semaphore_signal(barrier, inc=1, device_id=device, device_id_type=MESH)
    pl.semaphore_wait(barrier, len(devices))


def params(collective_id=None):
    more = {} if collective_id is None else {"collective_id": collective_id, "has_side_effects": True}
    return pltpu.CompilerParams(vmem_limit_bytes=60 * 1024 * 1024, **more)


def index_of(z, y, c):
    return (z * RING + y) * 2 + c


def coords_of(index):
    return {"sp_0": index // 16, "sp_1": lax.rem(index // 2, RING), "sp_2": lax.rem(index, 2)}


def project_kernel(x_ref, gain_ref, wa_ref, wb_ref, oa_ref, ob_ref, ga, gb, halo, normed, hs, hr, *sems):
    torus = Torus([(wa_ref, ga, "y"), (wb_ref, gb, "z")], sems, (1, 1))
    me = index_of(torus.z, torus.y, torus.c)
    later, earlier = coords_of(lax.rem(me + 1, 128)), coords_of(lax.rem(me + 127, 128))
    meet(torus.signals() + [later, earlier])
    span = x_ref.shape[1]
    torus.go(x_ref.at[:, pl.ds(span - HALO, HALO)], halo, hs, hr, later)
    torus.begin()
    rows = span + HALO

    def norm(values):
        wide = values.astype(F32)
        scale = lax.rsqrt(jnp.mean(wide * wide, axis=-1, keepdims=True) + EPS)
        return (wide * scale * gain_ref[...]).astype(BF16)

    for b in range(2):
        for r in range(0, span, 32):
            normed[b * rows + HALO + r:b * rows + HALO + r + 32] = norm(x_ref[b, r:r + 32])
    torus.arrived(halo, hs, hr)
    for b in range(2):
        normed[b * rows:b * rows + HALO] = norm(halo[b])
    torus.finish()
    depth = normed.shape[1]
    for g, o in ((ga, oa_ref), (gb, ob_ref)):
        o[...] = jnp.dot(normed[...], g[...].reshape(depth, g.shape[-1]), preferred_element_type=F32)


def project(x, gain, wa, wb):
    rows = 2 * (x.shape[1] + HALO)
    dma = pltpu.SemaphoreType.DMA
    return pl.pallas_call(
        project_kernel,
        out_shape=[jax.ShapeDtypeStruct((rows, w.shape[1]), F32) for w in (wa, wb)],
        in_specs=[VMEM] * 4,
        out_specs=[VMEM] * 2,
        scratch_shapes=[
            *[pltpu.VMEM((8, 8, 2, *w.shape), BF16) for w in (wa, wb)],
            pltpu.VMEM((2, HALO, x.shape[2]), BF16),
            pltpu.VMEM((rows, x.shape[2]), BF16),
            dma,
            dma,
            *torus_sems(2, 1),
        ],
        compiler_params=params(0),
    )(x, gain, wa, wb)


def head_scale(values, gain):
    return values * lax.rsqrt(jnp.mean(values * values, axis=-1, keepdims=True) + EPS) * gain


def softplus(values):
    grown = jnp.exp(-jnp.abs(values))
    series = jnp.zeros_like(grown)
    for n in range(8, 0, -1):
        series = grown * ((1.0 if n % 2 else -1.0) / n + series)
    return jnp.maximum(values, 0.0) + jnp.where(grown < 0.06, series, jnp.log(1.0 + grown))


def one_less_exp(values):
    series = jnp.zeros_like(values)
    for n in range(8, 0, -1):
        series = values / n * (1.0 + series)
    return jnp.where(values > -0.3, -series, 1.0 - jnp.exp(values))


def local_kernel(
    oa_ref, ob_ref, qg_ref, kg_ref, cw_ref, dw_ref, iw_ref, dp_ref, de_ref, q_ref, k0_ref, k1_ref, cum_ref, loc_ref, sum_ref
):
    span = q_ref.shape[1] // 4
    rows = span + HALO
    me = lax.axis_index(SP)
    lane = lax.broadcasted_iota(jnp.int32, (span, 16), 1)
    power = softplus(-dp_ref[...]) * -8.0
    for b, k_ref in enumerate((k0_ref, k1_ref)):
        own = pl.ds(b * rows + HALO, span)
        proj = oa_ref[own, :256]
        for h in range(4):
            q = head_scale(proj[:, h * 64:(h + 1) * 64], qg_ref[...]).astype(BF16).astype(F32) * 0.125
            picks = jnp.where((lane % 4 == h) & (lane < 12), 1.0, 0.0)
            q_ref[b, h * span:(h + 1) * span] = jnp.concatenate([q, picks], axis=1).astype(BF16)
        kv = ob_ref[own, :128]
        key = head_scale(kv[:, :64], kg_ref[...])
        k_ref[...] = jnp.concatenate([key, kv[:, 64:]], axis=1).T.astype(BF16)
        before = oa_ref[b * rows:b * rows + HALO, 256:] * jnp.where(me > 0, 1.0, 0.0)
        ext = jnp.concatenate([before, oa_ref[own, 256:]], axis=0).astype(BF16).astype(F32)
        conv = jnp.zeros((span, 256), F32)
        for k in range(4):
            conv = conv + ext[HALO - 3 + k:HALO - 3 + k + span] * cw_ref[k:k + 1].astype(F32)
        conv = conv.astype(BF16)
        gd, gi = (
            jnp.concatenate(
                [jnp.dot(conv[:, n * 64:(n + 1) * 64], w[n], preferred_element_type=F32) for n in range(4)], axis=1
            )
            for w in (dw_ref, iw_ref)
        )
        log_decay = power * jax.nn.sigmoid(gd) + de_ref[b]
        add = jnp.sqrt(one_less_exp(2.0 * log_decay)) * jax.nn.sigmoid(gi) * conv.astype(F32)
        mul = jnp.exp(log_decay)
        s = 1
        while s < span:
            mul_b = jnp.concatenate([jnp.ones((s, 256), F32), mul[:-s]], axis=0)
            add_b = jnp.concatenate([jnp.zeros((s, 256), F32), add[:-s]], axis=0)
            add = mul * add_b + add
            mul = mul * mul_b
            s *= 2
        cum_ref[b] = mul
        loc_ref[b] = add
        sum_ref[0, b:b + 1] = mul[span - 1:]
        sum_ref[1, b:b + 1] = add[span - 1:]


def local(oa, ob, *more):
    span = oa.shape[0] // 2 - HALO
    shape = jax.ShapeDtypeStruct
    return pl.pallas_call(
        local_kernel,
        out_shape=[
            shape((2, 4 * span, 80), BF16),
            *[shape((128, span), BF16)] * 2,
            *[shape((2, span, 256), F32)] * 2,
            shape((2, 2, 256), F32),
        ],
        in_specs=[VMEM] * 9,
        out_specs=[VMEM] * 6,
        compiler_params=params(),
    )(oa, ob, *more)


def gather_kernel(firsts, subs, *refs):
    n = len(firsts)
    torus = Torus([(refs[k], refs[n + k], firsts[k]) for k in range(n)], refs[2 * n:], subs)
    meet(torus.signals())
    torus.begin()
    torus.finish()


def torus_gather(arrays, firsts, subs, collective_id):
    return pl.pallas_call(
        functools.partial(gather_kernel, firsts, subs),
        out_shape=[jax.ShapeDtypeStruct((8, 8, 2, *a.shape), a.dtype) for a in arrays],
        in_specs=[VMEM] * len(arrays),
        out_specs=[VMEM] * len(arrays),
        scratch_shapes=torus_sems(len(arrays), max(subs)),
        compiler_params=params(collective_id),
    )(*arrays)


def gate_pieces(rel):
    hi = rel.astype(BF16).astype(F32)
    mid = (rel - hi).astype(BF16).astype(F32)
    return jnp.concatenate([hi, mid, rel - hi - mid, jnp.zeros_like(rel)], axis=0).astype(BF16)


CB = 32


def mix_kernel(
    q_ref, k0_ref, k1_ref, kv0_ref, kv1_ref, forget_ref, ag_ref, cum_ref, loc_ref, st_ref, ob_ref, rg_ref, wa_ref, wr_ref,
    out_ref, gates, acc, top, normed
):
    seqs, rows, depth = q_ref.shape
    span = k0_ref.shape[1]
    heads = rows // span
    owns, kvs = (k0_ref, k1_ref), (kv0_ref, kv1_ref)
    me = lax.axis_index(SP)
    first = pl.multiple_of(me * span, span)
    chunk = CB * span
    ones_own = jnp.ones((16, span), BF16)
    ones = jnp.ones((16, chunk), BF16)
    row = lax.broadcasted_iota(jnp.int32, (rows, span), 0) % span
    col = lax.broadcasted_iota(jnp.int32, (rows, span), 1)
    count = (me + CB - 1) // CB
    for b in range(seqs):
        near = forget_ref[b, :, pl.ds(first, span)]
        base = near[:, :1]

        def prep(c, _):
            at = pl.multiple_of(c * chunk, chunk)
            rel = base - forget_ref[b, :, pl.ds(at, chunk)]
            pos = at + lax.broadcasted_iota(jnp.int32, rel.shape, 1)
            gates[b, :, pl.ds(at, chunk)] = gate_pieces(jnp.where(pos < first, rel, -1e30))
            return 0

        lax.fori_loop(0, count, prep, 0)
        own = owns[b][...]
        rhs = jnp.concatenate([own[:64], gate_pieces(base - near)], axis=0)
        s = jnp.dot(q_ref[b], rhs, preferred_element_type=F32)
        s = jnp.where(row >= col, s, -jnp.inf)
        m = jnp.max(s, axis=1, keepdims=True)
        p = jnp.exp(s - m).astype(BF16)
        acc[b] = lax.dot_general(p, jnp.concatenate([own[64:], ones_own], axis=0), NT, preferred_element_type=F32)
        top[b] = jnp.broadcast_to(m, (rows, 128))

    def work(c, _):
        at = pl.multiple_of(c * chunk, chunk)
        for b in range(seqs):
            blocks = [kvs[b][c * CB + i] for i in range(CB)]
            kt = jnp.concatenate([x[:64] for x in blocks], axis=1)
            vt = jnp.concatenate([x[64:] for x in blocks], axis=1)
            rhs = jnp.concatenate([kt, gates[b, :, pl.ds(at, chunk)]], axis=0)
            s = jnp.dot(q_ref[b], rhs, preferred_element_type=F32)
            old = top[b][:, :1]
            m = jnp.maximum(old, jnp.max(s, axis=1, keepdims=True))
            p = jnp.exp(s - m).astype(BF16)
            vx = jnp.concatenate([vt, ones], axis=0)
            acc[b] = acc[b] * jnp.exp(old - m) + lax.dot_general(p, vx, NT, preferred_element_type=F32)
            top[b] = jnp.broadcast_to(m, (rows, 128))
        return 0

    lax.fori_loop(0, count, work, 0)

    def merge(j, state):
        return st_ref[j, 0] * state + st_ref[j, 1]

    entering = lax.fori_loop(0, me, merge, jnp.zeros((2, 256), F32))
    wide_rows = span + HALO
    for b in range(seqs):
        a = acc[b]
        att = head_scale(a[:, :64] / a[:, 64:65], 1.0)
        att = jnp.concatenate([att[h * span:(h + 1) * span] for h in range(heads)], axis=1)
        normed[0, b * span:(b + 1) * span] = (att * ag_ref[...]).astype(BF16)
        state = loc_ref[b] + cum_ref[b] * entering[b:b + 1]
        gated = state * jax.nn.gelu(ob_ref[pl.ds(b * wide_rows + HALO, span), 128:])
        rec = jnp.concatenate([head_scale(gated[:, n * 64:(n + 1) * 64], 1.0) for n in range(4)], axis=1)
        normed[1, b * span:(b + 1) * span] = (rec * rg_ref[...]).astype(BF16)
    width = out_ref.shape[2]
    for p in range(4):
        part = pl.ds(p * width, width)
        terms = jnp.dot(normed[0], wa_ref[:, part], preferred_element_type=F32)
        out_ref[p] = (terms + jnp.dot(normed[1], wr_ref[:, part], preferred_element_type=F32)).astype(BF16)


def mix(q, k0, k1, kv0, kv1, forget, *more):
    span, length = k0.shape[1], forget.shape[2]
    rows = q.shape[1]
    return pl.pallas_call(
        mix_kernel,
        out_shape=jax.ShapeDtypeStruct((4, 2 * span, more[-1].shape[1] // 4), BF16),
        in_specs=[VMEM] * (6 + len(more)),
        out_specs=VMEM,
        scratch_shapes=[
            pltpu.VMEM((2, 16, length), BF16),
            pltpu.VMEM((2, rows, 80), F32),
            pltpu.VMEM((2, rows, 128), F32),
            pltpu.VMEM((2, 2 * span, 256), BF16),
        ],
        compiler_params=params(),
    )(q, k0, k1, kv0, kv1, forget, *more)


def sum_kernel(terms_ref, out_ref, held, send, recv):
    me = lax.axis_index("tp")
    peers = [lax.rem(me + j, 4) for j in range(4)]
    meet([{"tp": p} for p in peers[1:]])
    copies = []
    for j in (2, 1, 3):
        copy = pltpu.make_async_remote_copy(
            src_ref=terms_ref.at[peers[j]], dst_ref=held.at[j - 1], send_sem=send.at[j - 1], recv_sem=recv.at[j - 1],
            device_id={"tp": peers[j]}, device_id_type=MESH,
        )
        copy.start()
        copies.append(copy)
    for copy in copies:
        copy.wait()
    total = terms_ref[me].astype(F32)
    for j in range(3):
        total = total + held[j].astype(F32)
    out_ref[...] = total.astype(BF16)


def summed(terms):
    dma = pltpu.SemaphoreType.DMA
    return pl.pallas_call(
        sum_kernel,
        out_shape=jax.ShapeDtypeStruct(terms.shape[1:], BF16),
        in_specs=[VMEM],
        out_specs=VMEM,
        scratch_shapes=[pltpu.VMEM((3, *terms.shape[1:]), BF16), dma((3,)), dma((3,))],
        compiler_params=params(2),
    )(terms)


def body(
    inputs, norm_gain, query_weight, key_weight, value_weight, query_gain, key_gain, forget_cache, rec_in_weight,
    rec_gate_weight, conv_weight, decay_gate_weight, input_gate_weight, decay_param, decay_extra, attn_out_gain,
    rec_out_gain, out_att_weight, out_rec_weight,
):
    span = inputs.shape[1]
    wa = jnp.concatenate([query_weight, rec_in_weight], axis=1)
    wb = jnp.concatenate([key_weight, value_weight, rec_gate_weight], axis=1)
    oa, ob = project(inputs, norm_gain[None], wa, wb)
    q, k0, k1, cum, loc, ends = local(
        oa, ob, query_gain[None], key_gain[None], conv_weight, decay_gate_weight, input_gate_weight, decay_param[None],
        decay_extra,
    )
    kv0, kv1, states = torus_gather([k0, k1, ends], ("y", "z", "y"), (2, 2, 1), 1)
    terms = mix(
        q, k0, k1, kv0.reshape(-1, *k0.shape), kv1.reshape(-1, *k1.shape), forget_cache, attn_out_gain[None], cum, loc,
        states.reshape(-1, *ends.shape), ob, rec_out_gain[None], out_att_weight, out_rec_weight,
    )
    return summed(terms).reshape(2, span, -1)


def solution(mesh):
    finer = Mesh(mesh.devices.reshape(8, 8, 2, mesh.shape["tp"]), (*SP, "tp"))
    return jax.shard_map(
        body,
        mesh=finer,
        in_specs=(
            P(None, SP, None), P(), P(SP, "tp"), P(SP, "tp"), P(SP, "tp"), P(), P(), P(None, "tp", None), P(SP, "tp"),
            P(SP, "tp"), P(None, "tp"), P("tp", None, None), P("tp", None, None), P("tp"), P(None, SP, "tp"), P("tp"),
            P("tp"), P("tp", None), P("tp", None),
        ),
        out_specs=P(None, SP, "tp"),
        check_vma=False,
    )
```

time: 241 us -> 154 us (0.64)
  the two profiles are of different devices: /device:TPU:448 before, /device:TPU:449 now
where the time goes in v2:
time: 154 us; the launch traced here: 153 us
  Pallas kernels  149 us (97%)
  other arithmetic  2.71 us (2%)
  local copies, waits for them, and re-layouts  1.67 us (1%)
    pallas_call x1, Pallas kernels, torus_gather(): pl.pallas_call(functools.partial(gather_kernel, firsts, subs), out_shape=...  49.7 us
    pallas_call x1, Pallas kernels, project(): pl.pallas_call(project_kernel, out_shape=[jax.ShapeDtypeStruct((rows, w.s...  42.2 us
    pallas_call x1, Pallas kernels, mix(): pl.pallas_call(mix_kernel, out_shape=jax.ShapeDtypeStruct((4, 2 * span, m...  34 us
    pallas_call x1, Pallas kernels, summed(): pl.pallas_call(sum_kernel, out_shape=jax.ShapeDtypeStruct(terms.shape[1:]...  18.7 us
    pallas_call x1, Pallas kernels, local(): pl.pallas_call(local_kernel, out_shape=[shape((2, 4 * span, 80), BF16), *...  4.22 us

profile of v2, /device:TPU:449, one launch (start us, length us, event | category | flops | bytes accessed | tf_op | source)
XLA Modules:
  0.0 153.2 jit_solution(18434319105930771845)
XLA Ops:
  0.0 1.4 pad_maximum_fusion.1.wb_ref
  1.4 1.3 pad_maximum_fusion.wa_ref
  2.7 42.2 %shard_map.181 = (f32[288,512]{1,0:T(8,128)}, f32[288,384]{1,0:T(8,128)}) custom-call(bf16[2,128,2048]{2,1,0:T(8,128)(2,1)} %x_ref.1, f32[1,2048]{1,0:T(1,128)} %bitcast.14, bf16[16,512]{1,0:T(8,128)(2,1)} %pad_maximum_fusion.wa_ref, bf16[16,384]{1,0:T(8,128)(2,1)} %pad_maximum_fusion.1.wb_ref), custom_call_target="tpu_custom_call" | custom-call | tf_op jit(solution)/shard_map/pallas_call | solution.py:198
  44.9 4.2 %shard_map.182 = (bf16[2,512,80]{2,1,0:T(8,128)(2,1)}, bf16[128,128]{1,0:T(8,128)(2,1)}, bf16[128,128]{1,0:T(8,128)(2,1)}, f32[2,128,256]{2,1,0:T(8,128)}, f32[2,128,256]{2,1,0:T(8,128)}, /*index=5*/f32[2,2,256]{2,1,0:T(2,128)}) custom-call(f32[288,512]{1,0:T(8,128)} %get-tuple-element.16.oa_ref, f32[288,384]{1,0:T(8,128)} %get-tuple-element.17.ob_ref, ...), custom_call_target="tpu_custom_call" | custom-call | tf_op jit(solution)/shard_map/pallas_call | solution.py:283
  49.1 49.7 %shard_map.183 = (bf16[8,8,2,128,128]{4,3,2,1,0:T(8,128)(2,1)}, bf16[8,8,2,128,128]{4,3,2,1,0:T(8,128)(2,1)}, f32[8,8,2,2,2,256]{5,4,3,2,1,0:T(2,128)}) custom-call(bf16[128,128]{1,0:T(8,128)(2,1)} %get-tuple-element.19.refs_0_.k0_ref, bf16[128,128]{1,0:T(8,128)(2,1)} %get-tuple-element.20.refs_1_.k1_ref, f32[2,2,256]{2,1,0:T(2,128)} %get-tuple-element.21.refs_2_), custom_call_target="tpu_custom_call" | custom-call | tf_op jit(solution)/shard_map/pallas_call | solution.py:306
  98.9 34.0 %shard_map.184.terms_ref = bf16[4,256,512]{2,1,0:T(8,128)(2,1)} custom-call(bf16[2,512,80]{2,1,0:T(8,128)(2,1)} %get-tuple-element.18.q_ref, bf16[128,128]{1,0:T(8,128)(2,1)} %get-tuple-element.19.refs_0_.k0_ref, bf16[128,128]{1,0:T(8,128)(2,1)} %get-tuple-element.20.refs_1_.k1_ref, bf16[128,128,128]{2,1,0:T(8,128)(2,1)} %bitcast.10, ...), custom_call_target="tpu_custom_call" | custom-call | tf_op jit(solution)/shard_map/pallas_call | solution.py:404
  132.9 18.7 %shard_map.185 = bf16[256,512]{1,0:T(8,128)(2,1)} custom-call(bf16[4,256,512]{2,1,0:T(8,128)(2,1)} %shard_map.184.terms_ref), custom_call_target="tpu_custom_call" | custom-call | tf_op jit(solution)/shard_map/pallas_call | solution.py:441
  151.6 1.7 %copy.21 = bf16[2,128,512]{2,1,0:T(8,128)(2,1)} copy(bf16[2,128,512]{2,1,0:T(8,128)(2,1)} %bitcast.12) | data formatting | bytes 524288

commit v3 on v2

v3 whole, which is shorter than its diff:
```python
import functools

import jax
import jax.numpy as jnp
from jax import lax
from jax.experimental import pallas as pl
from jax.experimental.pallas import tpu as pltpu
from jax.sharding import Mesh
from jax.sharding import PartitionSpec as P

SP = ("sp_0", "sp_1", "sp_2")
NT = (((1,), (1,)), ((), ()))
EPS = 1e-6
HALO = 16
F32, BF16 = jnp.float32, jnp.bfloat16
VMEM = pl.BlockSpec(memory_space=pltpu.VMEM)

MESH = pl.DeviceIdType.MESH
RING = 8


class Torus:
    def __init__(self, streams, sems):
        self.streams = streams
        self.s1, self.r1, self.s2, self.r2, self.ps, self.pr = sems
        self.z, self.y, self.c = (lax.axis_index(n) for n in SP)
        self.sign = 1 - 2 * self.c
        self.other = {"sp_2": 1 - self.c}
        self.pending = []
        self.ks = range(len(streams))

    def peers(self):
        found = [self.other]
        for name, pos in (("sp_0", self.z), ("sp_1", self.y)):
            found += [{name: lax.rem(pos + i, RING)} for i in range(1, RING)]
        return found

    def places(self, k):
        return (self.y, self.z) if self.streams[k][2] == "y" else (self.z, self.y)

    def axes(self, k):
        return ("sp_1", "sp_0") if self.streams[k][2] == "y" else ("sp_0", "sp_1")

    def one(self, k, i):
        o, first = self.streams[k][1:]
        return o.at[self.z, i, self.c] if first == "y" else o.at[i, self.y, self.c]

    def line(self, k, j, core):
        o, first = self.streams[k][1:]
        return o.at[j, :, core] if first == "y" else o.at[:, j, core]

    def back(self, k, d, s):
        sg = self.sign if d == 0 else -self.sign
        return lax.rem(self.places(k)[1] - sg * s + RING, RING)

    def go(self, src, dst, send, recv, device):
        copy = pltpu.make_async_remote_copy(
            src_ref=src, dst_ref=dst, send_sem=send, recv_sem=recv, device_id=device, device_id_type=MESH
        )
        copy.start()
        self.pending.append(copy)

    def arrived(self, ref, send, recv):
        pltpu.make_async_remote_copy(
            src_ref=ref, dst_ref=ref, send_sem=send, recv_sem=recv, device_id=self.other, device_id_type=MESH
        ).wait_recv()

    def begin(self):
        for i in (4, 5, 3, 6, 2, 7, 1):
            for k in self.ks:
                pos = self.places(k)[0]
                self.go(
                    self.streams[k][0], self.one(k, pos), self.s1.at[k, i - 1], self.r1.at[k, i - 1],
                    {self.axes(k)[0]: lax.rem(pos + i, RING)},
                )
        for k in self.ks:
            self.streams[k][1][self.z, self.y, self.c] = self.streams[k][0][...]

    def pass_on(self, k, d, s):
        j = self.back(k, d, s - 1)
        ref = self.line(k, j, self.c)
        device = {self.axes(k)[1]: self.back(k, d, -1)}
        self.go(ref, ref, self.s2.at[k, d, s - 1], self.r2.at[k, d, s - 1], device)

    def share(self, k, d, s):
        ref = self.line(k, self.back(k, d, s), self.c)
        self.go(ref, ref, self.ps.at[k, d, s], self.pr.at[k, d, s], self.other)

    def shared(self, k, d, s):
        ref = self.line(k, self.back(k, d, -s), 1 - self.c)
        self.arrived(ref, self.ps.at[k, d, s], self.pr.at[k, d, s])

    def finish(self, work=lambda k, j: None):
        for k in self.ks:
            for i in range(1, RING):
                pos = self.places(k)[0]
                got = self.one(k, lax.rem(pos + RING - i, RING))
                self.arrived(got, self.s1.at[k, i - 1], self.r1.at[k, i - 1])
            for d in (0, 1):
                self.pass_on(k, d, 1)
            self.share(k, 0, 0)
        for k in self.ks:
            self.shared(k, 0, 0)
        for k in self.ks:
            work(k, self.places(k)[1])
        for s in range(1, 5):
            for k in self.ks:
                for d in (0, 1):
                    if s + d <= 4:
                        got = self.line(k, self.back(k, d, s), self.c)
                        self.arrived(got, self.s2.at[k, d, s - 1], self.r2.at[k, d, s - 1])
                        if s + d < 4:
                            self.pass_on(k, d, s + 1)
                        self.share(k, d, s)
            for k in self.ks:
                for d in (0, 1):
                    if s + d <= 4:
                        self.shared(k, d, s)
            for k in self.ks:
                for d in (0, 1):
                    if s + d <= 4:
                        work(k, self.back(k, d, s))
        for copy in self.pending:
            copy.wait_send()


def torus_sems(n):
    dma = pltpu.SemaphoreType.DMA
    return [dma((n, 7)), dma((n, 7)), dma((n, 2, 4)), dma((n, 2, 4)), dma((n, 2, 5)), dma((n, 2, 5))]


def meet(devices):
    barrier = pltpu.get_barrier_semaphore()
    for device in devices:
        pl.semaphore_signal(barrier, inc=1, device_id=device, device_id_type=MESH)
    pl.semaphore_wait(barrier, len(devices))


def params(collective_id=None):
    more = {} if collective_id is None else {"collective_id": collective_id, "has_side_effects": True}
    return pltpu.CompilerParams(vmem_limit_bytes=60 * 1024 * 1024, **more)


def index_of(z, y, c):
    return (z * RING + y) * 2 + c


def coords_of(index):
    return {"sp_0": index // 16, "sp_1": lax.rem(index // 2, RING), "sp_2": lax.rem(index, 2)}


def project_kernel(x_ref, gain_ref, w_ref, oa_ref, ob_ref, ga, gb, halo, normed, hs, hr, *sems):
    cut, width = ga.shape[-1], w_ref.shape[-1]
    torus = Torus([(w_ref.at[:, pl.ds(0, cut)], ga, "y"), (w_ref.at[:, pl.ds(cut, width - cut)], gb, "z")], sems)
    me = index_of(torus.z, torus.y, torus.c)
    later, earlier = coords_of(lax.rem(me + 1, 128)), coords_of(lax.rem(me + 127, 128))
    meet(torus.peers() + [later, earlier])
    span = x_ref.shape[1]
    torus.go(x_ref.at[:, pl.ds(span - HALO, HALO)], halo, hs, hr, later)
    torus.begin()
    rows = span + HALO

    def norm(values):
        wide = values.astype(F32)
        scale = lax.rsqrt(jnp.mean(wide * wide, axis=-1, keepdims=True) + EPS)
        return (wide * scale * gain_ref[...]).astype(BF16)

    for b in range(2):
        for r in range(0, span, 32):
            normed[b * rows + HALO + r:b * rows + HALO + r + 32] = norm(x_ref[b, r:r + 32])
    torus.arrived(halo, hs, hr)
    for b in range(2):
        normed[b * rows:b * rows + HALO] = norm(halo[b])
    torus.finish()
    depth = normed.shape[1]
    for g, o in ((ga, oa_ref), (gb, ob_ref)):
        o[...] = jnp.dot(normed[...], g[...].reshape(depth, g.shape[-1]), preferred_element_type=F32)


def project(x, gain, w, cut):
    rows = 2 * (x.shape[1] + HALO)
    dma = pltpu.SemaphoreType.DMA
    return pl.pallas_call(
        project_kernel,
        out_shape=[jax.ShapeDtypeStruct((rows, n), F32) for n in (cut, w.shape[1] - cut)],
        in_specs=[VMEM] * 3,
        out_specs=[VMEM] * 2,
        scratch_shapes=[
            *[pltpu.VMEM((8, 8, 2, w.shape[0], n), BF16) for n in (cut, w.shape[1] - cut)],
            pltpu.VMEM((2, HALO, x.shape[2]), BF16),
            pltpu.VMEM((rows, x.shape[2]), BF16),
            dma,
            dma,
            *torus_sems(2),
        ],
        compiler_params=params(0),
    )(x, gain, w)


def head_scale(values, gain):
    return values * lax.rsqrt(jnp.mean(values * values, axis=-1, keepdims=True) + EPS) * gain


def softplus(values):
    grown = jnp.exp(-jnp.abs(values))
    series = jnp.zeros_like(grown)
    for n in range(8, 0, -1):
        series = grown * ((1.0 if n % 2 else -1.0) / n + series)
    return jnp.maximum(values, 0.0) + jnp.where(grown < 0.06, series, jnp.log(1.0 + grown))


def one_less_exp(values):
    series = jnp.zeros_like(values)
    for n in range(8, 0, -1):
        series = values / n * (1.0 + series)
    return jnp.where(values > -0.3, -series, 1.0 - jnp.exp(values))


def local_kernel(
    oa_ref, ob_ref, qg_ref, kg_ref, cw_ref, dw_ref, iw_ref, dp_ref, de_ref, q_ref, k0_ref, k1_ref, cum_ref, loc_ref, sum_ref
):
    span = q_ref.shape[1] // 4
    rows = span + HALO
    me = lax.axis_index(SP)
    lane = lax.broadcasted_iota(jnp.int32, (span, 16), 1)
    power = softplus(-dp_ref[...]) * -8.0
    for b, k_ref in enumerate((k0_ref, k1_ref)):
        own = pl.ds(b * rows + HALO, span)
        proj = oa_ref[own, :256]
        for h in range(4):
            q = head_scale(proj[:, h * 64:(h + 1) * 64], qg_ref[...]).astype(BF16).astype(F32) * 0.125
            picks = jnp.where((lane % 4 == h) & (lane < 12), 1.0, 0.0)
            q_ref[b, h * span:(h + 1) * span] = jnp.concatenate([q, picks], axis=1).astype(BF16)
        kv = ob_ref[own, :128]
        key = head_scale(kv[:, :64], kg_ref[...])
        k_ref[...] = jnp.concatenate([key, kv[:, 64:]], axis=1).T.astype(BF16)
        before = oa_ref[b * rows:b * rows + HALO, 256:] * jnp.where(me > 0, 1.0, 0.0)
        ext = jnp.concatenate([before, oa_ref[own, 256:]], axis=0).astype(BF16).astype(F32)
        conv = jnp.zeros((span, 256), F32)
        for k in range(4):
            conv = conv + ext[HALO - 3 + k:HALO - 3 + k + span] * cw_ref[k:k + 1].astype(F32)
        conv = conv.astype(BF16)
        gd, gi = (
            jnp.concatenate(
                [jnp.dot(conv[:, n * 64:(n + 1) * 64], w[n], preferred_element_type=F32) for n in range(4)], axis=1
            )
            for w in (dw_ref, iw_ref)
        )
        log_decay = power * jax.nn.sigmoid(gd) + de_ref[b]
        add = jnp.sqrt(one_less_exp(2.0 * log_decay)) * jax.nn.sigmoid(gi) * conv.astype(F32)
        mul = jnp.exp(log_decay)
        s = 1
        while s < span:
            mul_b = jnp.concatenate([jnp.ones((s, 256), F32), mul[:-s]], axis=0)
            add_b = jnp.concatenate([jnp.zeros((s, 256), F32), add[:-s]], axis=0)
            add = mul * add_b + add
            mul = mul * mul_b
            s *= 2
        cum_ref[b] = mul
        loc_ref[b] = add
        sum_ref[0, b:b + 1] = mul[span - 1:]
        sum_ref[1, b:b + 1] = add[span - 1:]


def local(oa, ob, *more):
    span = oa.shape[0] // 2 - HALO
    shape = jax.ShapeDtypeStruct
    return pl.pallas_call(
        local_kernel,
        out_shape=[
            shape((2, 4 * span, 80), BF16),
            *[shape((128, span), BF16)] * 2,
            *[shape((2, span, 256), F32)] * 2,
            shape((2, 2, 256), F32),
        ],
        in_specs=[VMEM] * 9,
        out_specs=[VMEM] * 6,
        compiler_params=params(),
    )(oa, ob, *more)


def gate_pieces(rel):
    hi = rel.astype(BF16).astype(F32)
    mid = (rel - hi).astype(BF16).astype(F32)
    return jnp.concatenate([hi, mid, rel - hi - mid, jnp.zeros_like(rel)], axis=0).astype(BF16)


def mix_kernel(
    k0_ref, k1_ref, ends_ref, q_ref, forget_ref, ag_ref, cum_ref, loc_ref, ob_ref, rg_ref, wa_ref, wr_ref, out_ref,
    kv0, kv1, st, gates, acc, top, normed, terms, held, send, recv, *sems
):
    seqs, rows, depth = q_ref.shape
    span = k0_ref.shape[1]
    heads = rows // span
    torus = Torus([(k0_ref, kv0, "y"), (k1_ref, kv1, "z"), (ends_ref, st, "y")], sems)
    column = lax.axis_index("tp")
    peers = [lax.rem(column + j, 4) for j in range(4)]
    meet(torus.peers() + [{"tp": p} for p in peers[1:]])
    torus.begin()
    me = index_of(torus.z, torus.y, torus.c)
    first = pl.multiple_of(me * span, span)
    line = 16 * span
    ones_own = jnp.ones((16, span), BF16)
    ones = jnp.ones((16, line), BF16)
    row = lax.broadcasted_iota(jnp.int32, (rows, span), 0) % span
    col = lax.broadcasted_iota(jnp.int32, (rows, span), 1)
    for b, k_ref in enumerate((k0_ref, k1_ref)):
        near = forget_ref[b, :, pl.ds(first, span)]
        base = near[:, :1]

        def prep(c, _):
            at = pl.multiple_of(c * line, line)
            rel = base - forget_ref[b, :, pl.ds(at, line)]
            pos = at + lax.broadcasted_iota(jnp.int32, rel.shape, 1)
            gates[b, :, pl.ds(at, line)] = gate_pieces(jnp.where(pos < first, rel, -1e30))
            return 0

        lax.fori_loop(0, RING, prep, 0)
        own = k_ref[...]
        rhs = jnp.concatenate([own[:64], gate_pieces(base - near)], axis=0)
        s = jnp.dot(q_ref[b], rhs, preferred_element_type=F32)
        s = jnp.where(row >= col, s, -jnp.inf)
        m = jnp.max(s, axis=1, keepdims=True)
        p = jnp.exp(s - m).astype(BF16)
        acc[b] = lax.dot_general(p, jnp.concatenate([own[64:], ones_own], axis=0), NT, preferred_element_type=F32)
        top[b] = jnp.broadcast_to(m, (rows, 128))

    def attend(b, blocks, near_gates):
        rhs = jnp.concatenate([jnp.concatenate([x[:64] for x in blocks], axis=1), near_gates], axis=0)
        s = jnp.dot(q_ref[b], rhs, preferred_element_type=F32)
        old = top[b][:, :1]
        m = jnp.maximum(old, jnp.max(s, axis=1, keepdims=True))
        p = jnp.exp(s - m).astype(BF16)
        vx = jnp.concatenate([jnp.concatenate([x[64:] for x in blocks], axis=1), ones], axis=0)
        acc[b] = acc[b] * jnp.exp(old - m) + lax.dot_general(p, vx, NT, preferred_element_type=F32)
        top[b] = jnp.broadcast_to(m, (rows, 128))

    def work(k, j):
        if k == 0:
            @pl.when(j * 16 < me)
            def _():
                attend(0, [kv0[j, i // 2, i % 2] for i in range(16)], gates[0, :, pl.ds(pl.multiple_of(j * line, line), line)])
        if k == 1:
            @pl.when(j * 2 < me)
            def _():
                parts = [gates[1, :, pl.ds(pl.multiple_of((z * RING + j) * 2 * span, 2 * span), 2 * span)] for z in range(RING)]
                attend(1, [kv1[i // 2, j, i % 2] for i in range(16)], jnp.concatenate(parts, axis=1))

    torus.finish(work)

    def merge(j, state):
        part = st.at[j // 16, lax.rem(j // 2, RING), lax.rem(j, 2)]
        return part[0] * state + part[1]

    entering = lax.fori_loop(0, me, merge, jnp.zeros((2, 256), F32))
    wide_rows = span + HALO
    for b in range(seqs):
        a = acc[b]
        att = head_scale(a[:, :64] / a[:, 64:65], 1.0)
        att = jnp.concatenate([att[h * span:(h + 1) * span] for h in range(heads)], axis=1)
        normed[0, b * span:(b + 1) * span] = (att * ag_ref[...]).astype(BF16)
        state = loc_ref[b] + cum_ref[b] * entering[b:b + 1]
        gated = state * jax.nn.gelu(ob_ref[pl.ds(b * wide_rows + HALO, span), 128:])
        rec = jnp.concatenate([head_scale(gated[:, n * 64:(n + 1) * 64], 1.0) for n in range(4)], axis=1)
        normed[1, b * span:(b + 1) * span] = (rec * rg_ref[...]).astype(BF16)
    width = out_ref.shape[1]
    copies = []
    for j in (2, 1, 3, 0):
        part = pl.ds(pl.multiple_of(peers[j] * width, width), width)
        total = jnp.dot(normed[0], wa_ref[:, part], preferred_element_type=F32)
        total = total + jnp.dot(normed[1], wr_ref[:, part], preferred_element_type=F32)
        terms[j] = total.astype(BF16)
        if j:
            copy = pltpu.make_async_remote_copy(
                src_ref=terms.at[j], dst_ref=held.at[j - 1], send_sem=send.at[j - 1], recv_sem=recv.at[j - 1],
                device_id={"tp": peers[j]}, device_id_type=MESH,
            )
            copy.start()
            copies.append(copy)
    for copy in copies:
        copy.wait()
    total = terms[0].astype(F32)
    for j in range(3):
        total = total + held[j].astype(F32)
    out_ref[...] = total.astype(BF16)


def mix(k0, k1, ends, q, forget, *more):
    span, length = k0.shape[1], forget.shape[2]
    rows = q.shape[1]
    width = more[-1].shape[1] // 4
    dma = pltpu.SemaphoreType.DMA
    return pl.pallas_call(
        mix_kernel,
        out_shape=jax.ShapeDtypeStruct((2 * span, width), BF16),
        in_specs=[VMEM] * (5 + len(more)),
        out_specs=VMEM,
        scratch_shapes=[
            pltpu.VMEM((8, 8, 2, *k0.shape), BF16),
            pltpu.VMEM((8, 8, 2, *k1.shape), BF16),
            pltpu.VMEM((8, 8, 2, *ends.shape), F32),
            pltpu.VMEM((2, 16, length), BF16),
            pltpu.VMEM((2, rows, 80), F32),
            pltpu.VMEM((2, rows, 128), F32),
            pltpu.VMEM((2, 2 * span, 256), BF16),
            pltpu.VMEM((4, 2 * span, width), BF16),
            pltpu.VMEM((3, 2 * span, width), BF16),
            dma((3,)),
            dma((3,)),
            *torus_sems(3),
        ],
        compiler_params=params(1),
    )(k0, k1, ends, q, forget, *more)


def body(
    inputs, norm_gain, query_weight, key_weight, value_weight, query_gain, key_gain, forget_cache, rec_in_weight,
    rec_gate_weight, conv_weight, decay_gate_weight, input_gate_weight, decay_param, decay_extra, attn_out_gain,
    rec_out_gain, out_att_weight, out_rec_weight,
):
    span = inputs.shape[1]
    cut = query_weight.shape[1] + rec_in_weight.shape[1]
    joined = jnp.concatenate([query_weight, rec_in_weight, key_weight, value_weight, rec_gate_weight], axis=1)
    oa, ob = project(inputs, norm_gain[None], joined, cut)
    q, k0, k1, cum, loc, ends = local(
        oa, ob, query_gain[None], key_gain[None], conv_weight, decay_gate_weight, input_gate_weight, decay_param[None],
        decay_extra,
    )
    mixed = mix(
        k0, k1, ends, q, forget_cache, attn_out_gain[None], cum, loc, ob, rec_out_gain[None], out_att_weight,
        out_rec_weight,
    )
    return mixed.reshape(2, span, -1)


def solution(mesh):
    finer = Mesh(mesh.devices.reshape(8, 8, 2, mesh.shape["tp"]), (*SP, "tp"))
    return jax.shard_map(
        body,
        mesh=finer,
        in_specs=(
            P(None, SP, None), P(), P(SP, "tp"), P(SP, "tp"), P(SP, "tp"), P(), P(), P(None, "tp", None), P(SP, "tp"),
            P(SP, "tp"), P(None, "tp"), P("tp", None, None), P("tp", None, None), P("tp"), P(None, SP, "tp"), P("tp"),
            P("tp"), P("tp", None), P("tp", None),
        ),
        out_specs=P(None, SP, "tp"),
        check_vma=False,
    )
```

time: 154 us -> 122 us (0.79)
  the two profiles are of different devices: /device:TPU:449 before, /device:TPU:1 now
where the time goes in v3:
time: 122 us
  Pallas kernels  118 us (97%)
  local copies, waits for them, and re-layouts  3.8 us (3%)
    pallas_call x1, Pallas kernels, mix(): pl.pallas_call(mix_kernel, out_shape=jax.ShapeDtypeStruct((2 * span, widt...  69.8 us
    pallas_call x1, Pallas kernels, project(): pl.pallas_call(project_kernel, out_shape=[jax.ShapeDtypeStruct((rows, n),...  44.3 us
    pallas_call x1, Pallas kernels, local(): pl.pallas_call(local_kernel, out_shape=[shape((2, 4 * span, 80), BF16), *...  4.22 us

profile of v3, /device:TPU:1, one launch (start us, length us, event | category | flops | bytes accessed | tf_op | source)
XLA Modules:
  0.0 122.1 jit_solution(16224109350470988999)
XLA Ops:
  0.0 0.0 copy-start
  0.0 0.7 copy-done
  0.7 1.4 %concatenate.3.w_ref = bf16[16,896]{1,0:T(8,128)(2,1)} concatenate(bf16[16,256]{1,0:T(8,128)(2,1)S(1)} %copy-done, bf16[16,256]{1,0:T(8,128)(2,1)} %param.27, bf16[16,64]{1,0:T(8,128)(2,1)} %param.22, bf16[16,64]{1,0:T(8,128)(2,1)} %param.23, bf16[16,256]{1,0:T(8,128)(2,1)} %param.28), dimensions={1} | concatenate | bytes 57344 | tf_op jit(solution)/shard_map/concatenate | solution.py:423
  2.1 44.3 %shard_map.181 = (f32[288,512]{1,0:T(8,128)}, f32[288,384]{1,0:T(8,128)}) custom-call(bf16[2,128,2048]{2,1,0:T(8,128)(2,1)} %x_ref.1, f32[1,2048]{1,0:T(1,128)} %bitcast.8, bf16[16,896]{1,0:T(8,128)(2,1)} %concatenate.3.w_ref), custom_call_target="tpu_custom_call" | custom-call | tf_op jit(solution)/shard_map/pallas_call | solution.py:183
  46.4 4.2 %shard_map.182 = (bf16[2,512,80]{2,1,0:T(8,128)(2,1)}, bf16[128,128]{1,0:T(8,128)(2,1)}, bf16[128,128]{1,0:T(8,128)(2,1)}, f32[2,128,256]{2,1,0:T(8,128)}, f32[2,128,256]{2,1,0:T(8,128)}, /*index=5*/f32[2,2,256]{2,1,0:T(2,128)}) custom-call(f32[288,512]{1,0:T(8,128)} %get-tuple-element.13.oa_ref, f32[288,384]{1,0:T(8,128)} %get-tuple-element.14.ob_ref, ...), custom_call_target="tpu_custom_call" | custom-call | tf_op jit(solution)/shard_map/pallas_call | solution.py:268
  50.7 69.8 %shard_map.183 = bf16[256,512]{1,0:T(8,128)(2,1)} custom-call(bf16[128,128]{1,0:T(8,128)(2,1)} %get-tuple-element.15.k0_ref, bf16[128,128]{1,0:T(8,128)(2,1)} %get-tuple-element.16.k1_ref, f32[2,2,256]{2,1,0:T(2,128)} %get-tuple-element.17.ends_ref, bf16[2,512,80]{2,1,0:T(8,128)(2,1)} %get-tuple-element.18.q_ref, f32[2,4,16384]{2,1,0:T(4,128)} %forget_ref.1, ...), custom_call_target="tpu_custom_call" | custom-call | tf_op jit(solution)/shard_map/pallas_call | solution.py:393
  120.5 1.7 %copy.21 = bf16[2,128,512]{2,1,0:T(8,128)(2,1)} copy(bf16[2,128,512]{2,1,0:T(8,128)(2,1)} %bitcast.7) | data formatting | bytes 524288
Async XLA Ops:
  0.0 0.7 copy-start

commit v4 on v3

v4 whole, which is shorter than its diff:
```python
import functools

import jax
import jax.numpy as jnp
from jax import lax
from jax.experimental import pallas as pl
from jax.experimental.pallas import tpu as pltpu
from jax.sharding import Mesh
from jax.sharding import PartitionSpec as P

SP = ("sp_0", "sp_1", "sp_2")
NT = (((1,), (1,)), ((), ()))
EPS = 1e-6
HALO = 16
F32, BF16 = jnp.float32, jnp.bfloat16
VMEM = pl.BlockSpec(memory_space=pltpu.VMEM)

MESH = pl.DeviceIdType.MESH
RING = 8


class Torus:
    def __init__(self, streams, sems):
        self.streams = streams
        self.s1, self.r1, self.s2, self.r2, self.ps, self.pr = sems
        self.z, self.y, self.c = (lax.axis_index(n) for n in SP)
        self.sign = 1 - 2 * self.c
        self.other = {"sp_2": 1 - self.c}
        self.ks = range(len(streams))

    def peers(self):
        found = [self.other]
        for name, pos in (("sp_0", self.z), ("sp_1", self.y)):
            found += [{name: lax.rem(pos + i, RING)} for i in range(1, RING)]
        return found

    def places(self, k):
        return (self.y, self.z) if self.streams[k][2] == "y" else (self.z, self.y)

    def axes(self, k):
        return ("sp_1", "sp_0") if self.streams[k][2] == "y" else ("sp_0", "sp_1")

    def one(self, k, i):
        o, first = self.streams[k][1:]
        return o.at[self.z, i, self.c] if first == "y" else o.at[i, self.y, self.c]

    def line(self, k, j, core):
        o, first = self.streams[k][1:]
        return o.at[j, :, core] if first == "y" else o.at[:, j, core]

    def back(self, k, d, s):
        sg = self.sign if d == 0 else -self.sign
        return lax.rem(self.places(k)[1] - sg * s + RING, RING)

    def copy(self, src, dst, send, recv, device):
        return pltpu.make_async_remote_copy(
            src_ref=src, dst_ref=dst, send_sem=send, recv_sem=recv, device_id=device, device_id_type=MESH
        )

    def arrived(self, ref, send, recv):
        self.copy(ref, ref, send, recv, self.other).wait_recv()

    def begin(self):
        for i in (4, 5, 3, 6, 2, 7, 1):
            for k in self.ks:
                pos = self.places(k)[0]
                self.copy(
                    self.streams[k][0], self.one(k, pos), self.s1.at[k, i - 1], self.r1.at[k, i - 1],
                    {self.axes(k)[0]: lax.rem(pos + i, RING)},
                ).start()
        for k in self.ks:
            self.streams[k][1][self.z, self.y, self.c] = self.streams[k][0][...]

    def joined(self, k):
        pos = self.places(k)[0]
        for i in range(1, RING):
            got = self.one(k, lax.rem(pos + RING - i, RING))
            self.arrived(got, self.s1.at[k, i - 1], self.r1.at[k, i - 1])

    def pass_on(self, k, d, s):
        ref = self.line(k, self.back(k, d, s - 1), self.c)
        device = {self.axes(k)[1]: self.back(k, d, -1)}
        self.copy(ref, ref, self.s2.at[k, d, s - 1], self.r2.at[k, d, s - 1], device).start()

    def share(self, k, j, d, s):
        ref = self.line(k, j, self.c)
        self.copy(ref, ref, self.ps.at[k, d, s], self.pr.at[k, d, s], self.other).start()

    def shared(self, k, j, d, s):
        self.arrived(self.line(k, j, 1 - self.c), self.ps.at[k, d, s], self.pr.at[k, d, s])

    def lines(self):
        for k in self.ks:
            self.joined(k)
            for d in (0, 1):
                self.pass_on(k, d, 1)
            self.share(k, self.places(k)[1], 0, 0)

    def step(self, s):
        for k in self.ks:
            for d in (0, 1):
                if not isinstance(s, int) or s + d <= 4:
                    got = self.line(k, self.back(k, d, s), self.c)
                    self.arrived(got, self.s2.at[k, d, s - 1], self.r2.at[k, d, s - 1])
                    if isinstance(s, int):
                        if s + d < 4:
                            self.pass_on(k, d, s + 1)
                    else:
                        pl.when(s + d < 4)(functools.partial(self.pass_on, k, d, s + 1))
                    self.share(k, self.back(k, d, s), d, s)

    def step_shared(self, s):
        for k in self.ks:
            for d in (0, 1):
                if not isinstance(s, int) or s + d <= 4:
                    self.shared(k, self.back(k, d, -s), d, s)

    def own_shared(self):
        for k in self.ks:
            self.shared(k, self.places(k)[1], 0, 0)

    def drain(self):
        for k in self.ks:
            one, line = self.streams[k][0], self.line(k, self.places(k)[1], self.c)
            for i in range(7):
                self.copy(one, one, self.s1.at[k, i], self.r1.at[k, i], self.other).wait_send()
            self.copy(line, line, self.ps.at[k, 0, 0], self.pr.at[k, 0, 0], self.other).wait_send()
            for i in range(7):
                d, s = i // 4, i % 4
                self.copy(line, line, self.s2.at[k, d, s], self.r2.at[k, d, s], self.other).wait_send()
                self.copy(line, line, self.ps.at[k, d, s + 1], self.pr.at[k, d, s + 1], self.other).wait_send()

    def short_lines(self):
        for k in self.ks:
            self.joined(k)
            pos = self.places(k)[1]
            ref = self.line(k, pos, self.c)
            for i in (4, 5, 3, 6, 2, 7, 1):
                d, s = (i - 1) // 4, (i - 1) % 4
                device = {self.axes(k)[1]: lax.rem(pos + i, RING)}
                self.copy(ref, ref, self.s2.at[k, d, s], self.r2.at[k, d, s], device).start()
            self.share(k, pos, 0, 0)

    def short_finish(self):
        for k in self.ks:
            pos = self.places(k)[1]
            for i in (1, 7, 2, 6, 3, 5, 4):
                d, s = (i - 1) // 4, (i - 1) % 4
                j = lax.rem(pos + RING - i, RING)
                self.arrived(self.line(k, j, self.c), self.s2.at[k, d, s], self.r2.at[k, d, s])
                self.share(k, j, d, s + 1)
            self.shared(k, pos, 0, 0)
            for i in range(1, RING):
                self.shared(k, lax.rem(pos + RING - i, RING), (i - 1) // 4, (i - 1) % 4 + 1)


def torus_sems(n):
    dma = pltpu.SemaphoreType.DMA
    return [dma((n, 7)), dma((n, 7)), dma((n, 2, 4)), dma((n, 2, 4)), dma((n, 2, 5)), dma((n, 2, 5))]


def meet(devices):
    barrier = pltpu.get_barrier_semaphore()
    for device in devices:
        pl.semaphore_signal(barrier, inc=1, device_id=device, device_id_type=MESH)
    pl.semaphore_wait(barrier, len(devices))

def params(collective_id=None):
    more = {} if collective_id is None else {"collective_id": collective_id, "has_side_effects": True}
    return pltpu.CompilerParams(vmem_limit_bytes=60 * 1024 * 1024, **more)


def index_of(z, y, c):
    return (z * RING + y) * 2 + c


def coords_of(index):
    return {"sp_0": index // 16, "sp_1": lax.rem(index // 2, RING), "sp_2": lax.rem(index, 2)}


def head_scale(values, gain):
    return values * lax.rsqrt(jnp.mean(values * values, axis=-1, keepdims=True) + EPS) * gain


def softplus(values):
    grown = jnp.exp(-jnp.abs(values))
    series = jnp.zeros_like(grown)
    for n in range(8, 0, -1):
        series = grown * ((1.0 if n % 2 else -1.0) / n + series)
    return jnp.maximum(values, 0.0) + jnp.where(grown < 0.06, series, jnp.log(1.0 + grown))


def one_less_exp(values):
    series = jnp.zeros_like(values)
    for n in range(8, 0, -1):
        series = values / n * (1.0 + series)
    return jnp.where(values > -0.3, -series, 1.0 - jnp.exp(values))


def gate_pieces(rel):
    hi = rel.astype(BF16).astype(F32)
    mid = (rel - hi).astype(BF16).astype(F32)
    return jnp.concatenate([hi, mid, rel - hi - mid, jnp.zeros_like(rel)], axis=0).astype(BF16)


def kernel(
    x_ref, gain_ref, w_ref, qg_ref, kg_ref, cw_ref, dw_ref, iw_ref, dp_ref, de_ref, forget_ref, ag_ref, rg_ref, wa_ref,
    wr_ref, out_ref, gk, ga, gb, kv0, kv1, st, halo, normed, proj, k0_ref, k1_ref, ends, q_ref, gates, acc, top, cum, loc,
    mixed, terms, held, send, recv, hs, hr, *sems
):
    seqs, rows, depth = q_ref.shape
    span = k0_ref.shape[1]
    heads = rows // span
    wide = span + HALO
    ck, ca, cb = gk.shape[-1], ga.shape[-1], gb.shape[-1]
    first_w = Torus([(w_ref.at[:, pl.ds(0, ck)], gk, "y")], sems[:6])
    more_w = Torus([(w_ref.at[:, pl.ds(ck, ca)], ga, "y"), (w_ref.at[:, pl.ds(ck + ca, cb)], gb, "z")], sems[6:12])
    keys = Torus([(k0_ref, kv0, "y"), (k1_ref, kv1, "z")], sems[12:18])
    chain = Torus([(ends, st, "y")], sems[18:])
    me = index_of(keys.z, keys.y, keys.c)
    later, earlier = coords_of(lax.rem(me + 1, 128)), coords_of(lax.rem(me + 127, 128))
    column = lax.axis_index("tp")
    peers = [lax.rem(column + j, 4) for j in range(4)]
    meet(keys.peers() + [{"tp": p} for p in peers[1:]] + [later, earlier])
    first_w.begin()
    edge = keys.copy(x_ref.at[:, pl.ds(span - HALO, HALO)], halo, hs, hr, later)
    edge.start()
    more_w.begin()

    def norm(values):
        full = values.astype(F32)
        scale = lax.rsqrt(jnp.mean(full * full, axis=-1, keepdims=True) + EPS)
        return (full * scale * gain_ref[...]).astype(BF16)

    for b in range(seqs):
        for r in range(0, span, 32):
            normed[b * wide + HALO + r:b * wide + HALO + r + 32] = norm(x_ref[b, r:r + 32])
    first_w.short_lines()
    edge.wait()
    for b in range(seqs):
        normed[b * wide:b * wide + HALO] = norm(halo[b])
    more_w.lines()
    more_w.step(1)
    first_w.short_finish()
    kv_proj = jnp.dot(normed[...], gk[...].reshape(-1, ck), preferred_element_type=F32)
    for b, k_ref in enumerate((k0_ref, k1_ref)):
        kv = kv_proj[b * wide + HALO:(b + 1) * wide]
        k_ref[...] = jnp.concatenate([head_scale(kv[:, :64], kg_ref[...]), kv[:, 64:]], axis=1).T.astype(BF16)
    keys.begin()
    more_w.step(2)

    first = pl.multiple_of(me * span, span)
    line = 16 * span
    for b in range(seqs):
        base = forget_ref[b, :, pl.ds(first, span)][:, :1]

        def prep(c, _):
            at = pl.multiple_of(c * line, line)
            rel = base - forget_ref[b, :, pl.ds(at, line)]
            pos = at + lax.broadcasted_iota(jnp.int32, rel.shape, 1)
            gates[b, :, pl.ds(at, line)] = gate_pieces(jnp.where(pos < first, rel, -1e30))
            return 0

        lax.fori_loop(0, RING, prep, 0)
    more_w.step(3)
    keys.lines()
    more_w.step(4)
    more_w.own_shared()
    for s in range(1, 5):
        more_w.step_shared(s)
    for g, at, n in ((ga, 0, ca), (gb, ca, cb)):
        proj[:, at:at + n] = jnp.dot(normed[...], g[...].reshape(-1, n), preferred_element_type=F32)

    power = softplus(-dp_ref[...]) * -8.0
    for b in range(seqs):
        own = pl.ds(b * wide + HALO, span)
        before = proj[b * wide:b * wide + HALO, 256:512] * jnp.where(me > 0, 1.0, 0.0)
        ext = jnp.concatenate([before, proj[own, 256:512]], axis=0).astype(BF16).astype(F32)
        conv = jnp.zeros((span, 256), F32)
        for k in range(4):
            conv = conv + ext[HALO - 3 + k:HALO - 3 + k + span] * cw_ref[k:k + 1].astype(F32)
        conv = conv.astype(BF16)
        gd, gi = (
            jnp.concatenate(
                [jnp.dot(conv[:, n * 64:(n + 1) * 64], w[n], preferred_element_type=F32) for n in range(4)], axis=1
            )
            for w in (dw_ref, iw_ref)
        )
        log_decay = power * jax.nn.sigmoid(gd) + de_ref[b]
        add = jnp.sqrt(one_less_exp(2.0 * log_decay)) * jax.nn.sigmoid(gi) * conv.astype(F32)
        mul = jnp.exp(log_decay)
        s = 1
        while s < span:
            mul_b = jnp.concatenate([jnp.ones((s, 256), F32), mul[:-s]], axis=0)
            add_b = jnp.concatenate([jnp.zeros((s, 256), F32), add[:-s]], axis=0)
            add = mul * add_b + add
            mul = mul * mul_b
            s *= 2
        cum[b] = mul
        loc[b] = add
        ends[0, b:b + 1] = mul[span - 1:]
        ends[1, b:b + 1] = add[span - 1:]
    chain.begin()

    ones_own = jnp.ones((16, span), BF16)
    ones = jnp.ones((16, line), BF16)
    row = lax.broadcasted_iota(jnp.int32, (rows, span), 0) % span
    col = lax.broadcasted_iota(jnp.int32, (rows, span), 1)
    lane = lax.broadcasted_iota(jnp.int32, (span, 16), 1)
    for b, k_ref in enumerate((k0_ref, k1_ref)):
        query = proj[pl.ds(b * wide + HALO, span), :256]
        for h in range(heads):
            q = head_scale(query[:, h * 64:(h + 1) * 64], qg_ref[...]).astype(BF16).astype(F32) * 0.125
            picks = jnp.where((lane % 4 == h) & (lane < 12), 1.0, 0.0)
            q_ref[b, h * span:(h + 1) * span] = jnp.concatenate([q, picks], axis=1).astype(BF16)
        near = forget_ref[b, :, pl.ds(first, span)]
        own = k_ref[...]
        rhs = jnp.concatenate([own[:64], gate_pieces(near[:, :1] - near)], axis=0)
        s = jnp.dot(q_ref[b], rhs, preferred_element_type=F32)
        s = jnp.where(row >= col, s, -jnp.inf)
        m = jnp.max(s, axis=1, keepdims=True)
        p = jnp.exp(s - m).astype(BF16)
        acc[b] = lax.dot_general(p, jnp.concatenate([own[64:], ones_own], axis=0), NT, preferred_element_type=F32)
        top[b] = jnp.broadcast_to(m, (rows, 128))

    def attend(b, blocks, near_gates):
        rhs = jnp.concatenate([jnp.concatenate([x[:64] for x in blocks], axis=1), near_gates], axis=0)
        s = jnp.dot(q_ref[b], rhs, preferred_element_type=F32)
        old = top[b][:, :1]
        m = jnp.maximum(old, jnp.max(s, axis=1, keepdims=True))
        p = jnp.exp(s - m).astype(BF16)
        vx = jnp.concatenate([jnp.concatenate([x[64:] for x in blocks], axis=1), ones], axis=0)
        acc[b] = acc[b] * jnp.exp(old - m) + lax.dot_general(p, vx, NT, preferred_element_type=F32)
        top[b] = jnp.broadcast_to(m, (rows, 128))

    def work_0(j):
        @pl.when(j * 16 < me)
        def _():
            attend(0, [kv0[j, i // 2, i % 2] for i in range(16)], gates[0, :, pl.ds(pl.multiple_of(j * line, line), line)])

    def work_1(j):
        @pl.when(j * 2 < me)
        def _():
            parts = [gates[1, :, pl.ds(pl.multiple_of((z * RING + j) * 2 * span, 2 * span), 2 * span)] for z in range(RING)]
            attend(1, [kv1[i // 2, j, i % 2] for i in range(16)], jnp.concatenate(parts, axis=1))

    keys.step(1)
    keys.own_shared()
    work_0(keys.z)
    work_1(keys.y)
    chain.lines()

    for s in range(1, 4):
        keys.step_shared(s)

        def both(d, _):
            sg = keys.sign * (1 - 2 * d)
            work_0(lax.rem(keys.z - sg * s + RING, RING))
            work_1(lax.rem(keys.y - sg * s + RING, RING))
            return 0

        lax.fori_loop(0, 2, both, 0)
        keys.step(s + 1)
        chain.step(s)
    keys.step_shared(4)
    work_0(keys.back(0, 0, 4))
    work_1(keys.back(1, 0, 4))
    chain.step(4)
    chain.own_shared()
    for s in range(1, 5):
        chain.step_shared(s)

    def merge(j, state):
        part = st.at[j // 16, lax.rem(j // 2, RING), lax.rem(j, 2)]
        return part[0] * state + part[1]

    entering = lax.fori_loop(0, me, merge, jnp.zeros((2, 256), F32))
    for b in range(seqs):
        a = acc[b]
        att = head_scale(a[:, :64] / a[:, 64:65], 1.0)
        att = jnp.concatenate([att[h * span:(h + 1) * span] for h in range(heads)], axis=1)
        mixed[0, b * span:(b + 1) * span] = (att * ag_ref[...]).astype(BF16)
        state = loc[b] + cum[b] * entering[b:b + 1]
        gated = state * jax.nn.gelu(proj[pl.ds(b * wide + HALO, span), 512:])
        rec = jnp.concatenate([head_scale(gated[:, n * 64:(n + 1) * 64], 1.0) for n in range(4)], axis=1)
        mixed[1, b * span:(b + 1) * span] = (rec * rg_ref[...]).astype(BF16)
    width = out_ref.shape[1]
    copies = []
    for j in (2, 1, 3, 0):
        part = pl.ds(pl.multiple_of(peers[j] * width, width), width)
        total = jnp.dot(mixed[0], wa_ref[:, part], preferred_element_type=F32)
        total = total + jnp.dot(mixed[1], wr_ref[:, part], preferred_element_type=F32)
        terms[j] = total.astype(BF16)
        if j:
            copy = keys.copy(terms.at[j], held.at[j - 1], send.at[j - 1], recv.at[j - 1], {"tp": peers[j]})
            copy.start()
            copies.append(copy)
    for group in (first_w, more_w, keys, chain):
        group.drain()
    for copy in copies:
        copy.wait()
    total = terms[0].astype(F32)
    for j in range(3):
        total = total + held[j].astype(F32)
    out_ref[...] = total.astype(BF16)


def layer(x, gain, w, *more):
    span, length, out_cols = x.shape[1], more[7].shape[2], more[-1].shape[1]
    wide, width = 2 * (span + HALO), out_cols // 4
    dma = pltpu.SemaphoreType.DMA

    def grid(dtype, *shape):
        return pltpu.VMEM((8, 8, 2, *shape), dtype)

    return pl.pallas_call(
        kernel,
        out_shape=jax.ShapeDtypeStruct((2 * span, width), BF16),
        in_specs=[VMEM] * (3 + len(more)),
        out_specs=VMEM,
        scratch_shapes=[
            grid(BF16, w.shape[0], 128),
            grid(BF16, w.shape[0], 384),
            grid(BF16, w.shape[0], 384),
            grid(BF16, 128, span),
            grid(BF16, 128, span),
            grid(F32, 2, 2, 256),
            pltpu.VMEM((2, HALO, x.shape[2]), BF16),
            pltpu.VMEM((wide, x.shape[2]), BF16),
            pltpu.VMEM((wide, 768), F32),
            pltpu.VMEM((128, span), BF16),
            pltpu.VMEM((128, span), BF16),
            pltpu.VMEM((2, 2, 256), F32),
            pltpu.VMEM((2, 4 * span, 80), BF16),
            pltpu.VMEM((2, 16, length), BF16),
            pltpu.VMEM((2, 4 * span, 80), F32),
            pltpu.VMEM((2, 4 * span, 128), F32),
            pltpu.VMEM((2, span, 256), F32),
            pltpu.VMEM((2, span, 256), F32),
            pltpu.VMEM((2, 2 * span, 256), BF16),
            pltpu.VMEM((4, 2 * span, width), BF16),
            pltpu.VMEM((3, 2 * span, width), BF16),
            dma((3,)),
            dma((3,)),
            dma,
            dma,
            *torus_sems(1),
            *torus_sems(2),
            *torus_sems(2),
            *torus_sems(1),
        ],
        compiler_params=params(0),
    )(x, gain, w, *more)


def body(
    inputs, norm_gain, query_weight, key_weight, value_weight, query_gain, key_gain, forget_cache, rec_in_weight,
    rec_gate_weight, conv_weight, decay_gate_weight, input_gate_weight, decay_param, decay_extra, attn_out_gain,
    rec_out_gain, out_att_weight, out_rec_weight,
):
    joined = jnp.concatenate([key_weight, value_weight, query_weight, rec_in_weight, rec_gate_weight], axis=1)
    mixed = layer(
        inputs, norm_gain[None], joined, query_gain[None], key_gain[None], conv_weight, decay_gate_weight,
        input_gate_weight, decay_param[None], decay_extra, forget_cache, attn_out_gain[None], rec_out_gain[None],
        out_att_weight, out_rec_weight,
    )
    return mixed.reshape(2, inputs.shape[1], -1)


def solution(mesh):
    finer = Mesh(mesh.devices.reshape(8, 8, 2, mesh.shape["tp"]), (*SP, "tp"))
    return jax.shard_map(
        body,
        mesh=finer,
        in_specs=(
            P(None, SP, None), P(), P(SP, "tp"), P(SP, "tp"), P(SP, "tp"), P(), P(), P(None, "tp", None), P(SP, "tp"),
            P(SP, "tp"), P(None, "tp"), P("tp", None, None), P("tp", None, None), P("tp"), P(None, SP, "tp"), P("tp"),
            P("tp"), P("tp", None), P("tp", None),
        ),
        out_specs=P(None, SP, "tp"),
        check_vma=False,
    )
```

time: 122 us -> 111 us (0.910)
  Pallas kernels: 118 us -> 107 us
    pallas_call x3 -> x1, Pallas kernels: 118 us -> 107 us  [layer(): pl.pallas_call(kernel, out_shape=jax.ShapeDtypeStruct((2 * span, width),...]
where the time goes in v4:
time: 111 us; the launch traced here: 110 us
  Pallas kernels  107 us (96%)
  local copies, waits for them, and re-layouts  3.8 us (3%)
    pallas_call x1, Pallas kernels, layer(): pl.pallas_call(kernel, out_shape=jax.ShapeDtypeStruct((2 * span, width),...  107 us
    unnamed x3, local copies, waits for them, and re-layouts  2.37 us

profile of v4, /device:TPU:1, one launch (start us, length us, event | category | flops | bytes accessed | tf_op | source)
XLA Modules:
  0.0 110.4 jit_solution(11498728269475391905)
XLA Ops:
  0.0 0.0 copy-start
  0.0 0.7 copy-done
  0.7 1.4 %concatenate.3.w_ref = bf16[16,896]{1,0:T(8,128)(2,1)} concatenate(bf16[16,64]{1,0:T(8,128)(2,1)} %param.22, bf16[16,64]{1,0:T(8,128)(2,1)} %param.23, bf16[16,256]{1,0:T(8,128)(2,1)S(1)} %copy-done, bf16[16,256]{1,0:T(8,128)(2,1)} %param.27, bf16[16,256]{1,0:T(8,128)(2,1)} %param.28), dimensions={1} | concatenate | bytes 57344 | tf_op jit(solution)/shard_map/concatenate | solution.py:461
  2.1 106.5 %shard_map.181 = bf16[256,512]{1,0:T(8,128)(2,1)} custom-call(bf16[2,128,2048]{2,1,0:T(8,128)(2,1)} %x_ref.1, f32[1,2048]{1,0:T(1,128)} %bitcast.8, bf16[16,896]{1,0:T(8,128)(2,1)} %concatenate.3.w_ref, f32[1,64]{1,0:T(1,128)} %bitcast.12, f32[1,64]{1,0:T(1,128)} %bitcast.13, bf16[4,256]{1,0:T(4,128)(2,1)} %cw_ref.1, bf16[4,64,64]{2,1,0:T(8,128)(2,1)} %dw_ref.1, ...), custom_call_target="tpu_custom_call" | custom-call | tf_op jit(solution)/shard_map/pallas_call | solution.py:416
  108.7 1.7 %copy.21 = bf16[2,128,512]{2,1,0:T(8,128)(2,1)} copy(bf16[2,128,512]{2,1,0:T(8,128)(2,1)} %bitcast.7) | data formatting | bytes 524288
Async XLA Ops:
  0.0 0.7 copy-start

commit v5 on v4

--- a/solution.py
+++ b/solution.py
@@ -14,6 +14,7 @@
 HALO = 16
 F32, BF16 = jnp.float32, jnp.bfloat16
 VMEM = pl.BlockSpec(memory_space=pltpu.VMEM)
+ANY = pl.BlockSpec(memory_space=pl.ANY)
 
 MESH = pl.DeviceIdType.MESH
 RING = 8
@@ -204,8 +205,8 @@
 
 
 def kernel(
-    x_ref, gain_ref, w_ref, qg_ref, kg_ref, cw_ref, dw_ref, iw_ref, dp_ref, de_ref, forget_ref, ag_ref, rg_ref, wa_ref,
-    wr_ref, out_ref, gk, ga, gb, kv0, kv1, st, halo, normed, proj, k0_ref, k1_ref, ends, q_ref, gates, acc, top, cum, loc,
+    x_ref, gain_ref, w_ref, qg_ref, kg_ref, cw_ref, dw_ref, iw_ref, dp_ref, de_hbm, forget_ref, ag_ref, rg_ref, wa_hbm,
+    wr_hbm, out_ref, de_ref, wa_ref, wr_ref, ls, gk, ga, gb, kv0, kv1, st, halo, normed, proj, k0_ref, k1_ref, ends, q_ref, gates, acc, top, cum, loc,
     mixed, terms, held, send, recv, hs, hr, *sems
 ):
     seqs, rows, depth = q_ref.shape
@@ -219,6 +220,12 @@
     chain = Torus([(ends, st, "y")], sems[18:])
     me = index_of(keys.z, keys.y, keys.c)
     later, earlier = coords_of(lax.rem(me + 1, 128)), coords_of(lax.rem(me + 127, 128))
+    loads = [
+        pltpu.make_async_copy(a, b, ls.at[i])
+        for i, (a, b) in enumerate(((de_hbm, de_ref), (wa_hbm, wa_ref), (wr_hbm, wr_ref)))
+    ]
+    for load in loads:
+        load.start()
     column = lax.axis_index("tp")
     peers = [lax.rem(column + j, 4) for j in range(4)]
     meet(keys.peers() + [{"tp": p} for p in peers[1:]] + [later, earlier])
@@ -271,6 +278,7 @@
     for g, at, n in ((ga, 0, ca), (gb, ca, cb)):
         proj[:, at:at + n] = jnp.dot(normed[...], g[...].reshape(-1, n), preferred_element_type=F32)
 
+    loads[0].wait()
     power = softplus(-dp_ref[...]) * -8.0
     for b in range(seqs):
         own = pl.ds(b * wide + HALO, span)
@@ -323,8 +331,14 @@
         acc[b] = lax.dot_general(p, jnp.concatenate([own[64:], ones_own], axis=0), NT, preferred_element_type=F32)
         top[b] = jnp.broadcast_to(m, (rows, 128))
 
-    def attend(b, blocks, near_gates):
-        rhs = jnp.concatenate([jnp.concatenate([x[:64] for x in blocks], axis=1), near_gates], axis=0)
+    def attend(b, parts):
+        kv = (kv0, kv1)[b]
+        spots = [(j, i, c) if b == 0 else (i, j, c) for j, c in parts for i in range(RING)]
+        blocks = [kv[z, y, c] for z, y, c in spots]
+        near_gates = [gates[b, :, pl.ds(pl.multiple_of(index_of(z, y, c) * span, span), span)] for z, y, c in spots]
+        rhs = jnp.concatenate(
+            [jnp.concatenate([x[:64] for x in blocks], axis=1), jnp.concatenate(near_gates, axis=1)], axis=0
+        )
         s = jnp.dot(q_ref[b], rhs, preferred_element_type=F32)
         old = top[b][:, :1]
         m = jnp.maximum(old, jnp.max(s, axis=1, keepdims=True))
@@ -333,38 +347,39 @@
         acc[b] = acc[b] * jnp.exp(old - m) + lax.dot_general(p, vx, NT, preferred_element_type=F32)
         top[b] = jnp.broadcast_to(m, (rows, 128))
 
-    def work_0(j):
-        @pl.when(j * 16 < me)
-        def _():
-            attend(0, [kv0[j, i // 2, i % 2] for i in range(16)], gates[0, :, pl.ds(pl.multiple_of(j * line, line), line)])
-
-    def work_1(j):
-        @pl.when(j * 2 < me)
-        def _():
-            parts = [gates[1, :, pl.ds(pl.multiple_of((z * RING + j) * 2 * span, 2 * span), 2 * span)] for z in range(RING)]
-            attend(1, [kv1[i // 2, j, i % 2] for i in range(16)], jnp.concatenate(parts, axis=1))
-
+    def work(b, *parts):
+        near = [j * (16 if b == 0 else 2) < me for j, _ in parts]
+        pl.when(functools.reduce(jnp.logical_or, near))(lambda: attend(b, parts))
+
+    def sides(b, s, core):
+        work(b, *[(keys.back(b, d, s), core) for d in (0, 1)])
+
+    mine, its = keys.c, 1 - keys.c
     keys.step(1)
     keys.own_shared()
-    work_0(keys.z)
-    work_1(keys.y)
+    work(0, (keys.z, 0), (keys.z, 1))
+    work(1, (keys.y, 0), (keys.y, 1))
     chain.lines()
 
-    for s in range(1, 4):
+    def turn(s, _):
+        sides(0, s, mine)
+        sides(1, s, mine)
         keys.step_shared(s)
-
-        def both(d, _):
-            sg = keys.sign * (1 - 2 * d)
-            work_0(lax.rem(keys.z - sg * s + RING, RING))
-            work_1(lax.rem(keys.y - sg * s + RING, RING))
-            return 0
-
-        lax.fori_loop(0, 2, both, 0)
+        sides(0, s, its)
+        sides(1, s, its)
         keys.step(s + 1)
         chain.step(s)
+        return 0
+
+    lax.fori_loop(1, 3, turn, 0)
+    sides(0, 3, mine)
+    sides(1, 3, mine)
+    keys.step_shared(3)
+    sides(0, 3, its)
+    keys.step(4)
+    chain.step(3)
     keys.step_shared(4)
-    work_0(keys.back(0, 0, 4))
-    work_1(keys.back(1, 0, 4))
+    work(0, (keys.back(0, 0, 4), 0), (keys.back(0, 0, 4), 1))
     chain.step(4)
     chain.own_shared()
     for s in range(1, 5):
@@ -375,34 +390,56 @@
         return part[0] * state + part[1]
 
     entering = lax.fori_loop(0, me, merge, jnp.zeros((2, 256), F32))
-    for b in range(seqs):
+    width = out_ref.shape[1]
+    loads[1].wait()
+    loads[2].wait()
+    links = []
+
+    def post(i, src, j):
+        copy = keys.copy(src, held.at[i], send.at[i], recv.at[i], {"tp": peers[j]})
+        copy.start()
+        links.append(copy)
+
+    def products(b, straight):
         a = acc[b]
         att = head_scale(a[:, :64] / a[:, 64:65], 1.0)
         att = jnp.concatenate([att[h * span:(h + 1) * span] for h in range(heads)], axis=1)
-        mixed[0, b * span:(b + 1) * span] = (att * ag_ref[...]).astype(BF16)
+        mixed[0] = (att * ag_ref[...]).astype(BF16)
         state = loc[b] + cum[b] * entering[b:b + 1]
         gated = state * jax.nn.gelu(proj[pl.ds(b * wide + HALO, span), 512:])
         rec = jnp.concatenate([head_scale(gated[:, n * 64:(n + 1) * 64], 1.0) for n in range(4)], axis=1)
-        mixed[1, b * span:(b + 1) * span] = (rec * rg_ref[...]).astype(BF16)
-    width = out_ref.shape[1]
-    copies = []
-    for j in (2, 1, 3, 0):
-        part = pl.ds(pl.multiple_of(peers[j] * width, width), width)
-        total = jnp.dot(mixed[0], wa_ref[:, part], preferred_element_type=F32)
-        total = total + jnp.dot(mixed[1], wr_ref[:, part], preferred_element_type=F32)
-        terms[j] = total.astype(BF16)
-        if j:
-            copy = keys.copy(terms.at[j], held.at[j - 1], send.at[j - 1], recv.at[j - 1], {"tp": peers[j]})
-            copy.start()
-            copies.append(copy)
+        mixed[1] = (rec * rg_ref[...]).astype(BF16)
+        for j in (2, straight, 4 - straight, 0):
+            part = pl.ds(pl.multiple_of(peers[j] * width, width), width)
+            total = jnp.dot(mixed[0], wa_ref[:, part], preferred_element_type=F32)
+            total = total + jnp.dot(mixed[1], wr_ref[:, part], preferred_element_type=F32)
+            terms[b, j] = total.astype(BF16)
+            if j == 2:
+                post(3 * b, terms.at[b, 2], 4 - straight)
+            if j == straight:
+                post(3 * b + 1, terms.at[b, j], straight)
+
+    def relay(b, straight):
+        links[3 * b].wait_recv()
+        onward = terms[b, 4 - straight].astype(F32) + held[3 * b].astype(F32)
+        terms[b, 4 - straight] = onward.astype(BF16)
+        post(3 * b + 2, terms.at[b, 4 - straight], 4 - straight)
+
+    products(0, 3)
+    sides(1, 3, its)
+    relay(0, 3)
+    work(1, (keys.back(1, 0, 4), 0), (keys.back(1, 0, 4), 1))
+    products(1, 1)
+    relay(1, 1)
     for group in (first_w, more_w, keys, chain):
         group.drain()
-    for copy in copies:
-        copy.wait()
-    total = terms[0].astype(F32)
-    for j in range(3):
-        total = total + held[j].astype(F32)
-    out_ref[...] = total.astype(BF16)
+    for b in range(seqs):
+        for i in (1, 2):
+            links[3 * b + i].wait_recv()
+        total = terms[b, 0].astype(F32) + held[3 * b + 1].astype(F32) + held[3 * b + 2].astype(F32)
+        out_ref[b * span:(b + 1) * span] = total.astype(BF16)
+    for link in links:
+        link.wait_send()
 
 
 def layer(x, gain, w, *more):
@@ -416,9 +453,13 @@
     return pl.pallas_call(
         kernel,
         out_shape=jax.ShapeDtypeStruct((2 * span, width), BF16),
-        in_specs=[VMEM] * (3 + len(more)),
+        in_specs=[ANY if i in (9, 13, 14) else VMEM for i in range(15)],
         out_specs=VMEM,
         scratch_shapes=[
+            pltpu.VMEM((2, span, 256), F32),
+            pltpu.VMEM(more[-2].shape, BF16),
+            pltpu.VMEM(more[-1].shape, BF16),
+            dma((3,)),
             grid(BF16, w.shape[0], 128),
             grid(BF16, w.shape[0], 384),
             grid(BF16, w.shape[0], 384),
@@ -437,11 +478,11 @@
             pltpu.VMEM((2, 4 * span, 128), F32),
             pltpu.VMEM((2, span, 256), F32),
             pltpu.VMEM((2, span, 256), F32),
-            pltpu.VMEM((2, 2 * span, 256), BF16),
-            pltpu.VMEM((4, 2 * span, width), BF16),
-            pltpu.VMEM((3, 2 * span, width), BF16),
-            dma((3,)),
-            dma((3,)),
+            pltpu.VMEM((2, span, 256), BF16),
+            pltpu.VMEM((2, 4, span, width), BF16),
+            pltpu.VMEM((6, span, width), BF16),
+            dma((6,)),
+            dma((6,)),
             dma,
             dma,
             *torus_sems(1),

time: 111 us -> 104 us (0.937)
  Pallas kernels: 107 us -> 99.7 us
    pallas_call x1, Pallas kernels: 107 us -> 99.7 us  [layer(): pl.pallas_call(kernel, out_shape=jax.ShapeDtypeStruct((2 * span, width),...]
where the time goes in v5:
time: 104 us; the launch traced here: 103 us
  Pallas kernels  99.7 us (96%)
  local copies, waits for them, and re-layouts  3.8 us (4%)
    pallas_call x1, Pallas kernels, layer(): pl.pallas_call(kernel, out_shape=jax.ShapeDtypeStruct((2 * span, width),...  99.7 us
    unnamed x3, local copies, waits for them, and re-layouts  2.37 us

profile of v5, /device:TPU:1, one launch (start us, length us, event | category | flops | bytes accessed | tf_op | source)
XLA Modules:
  0.0 103.5 jit_solution(10927956087537457257)
XLA Ops:
  0.0 0.0 copy-start
  0.0 0.7 copy-done
  0.7 1.4 %concatenate.3.w_ref = bf16[16,896]{1,0:T(8,128)(2,1)} concatenate(bf16[16,64]{1,0:T(8,128)(2,1)} %param.22, bf16[16,64]{1,0:T(8,128)(2,1)} %param.23, bf16[16,256]{1,0:T(8,128)(2,1)S(1)} %copy-done, bf16[16,256]{1,0:T(8,128)(2,1)} %param.27, bf16[16,256]{1,0:T(8,128)(2,1)} %param.28), dimensions={1} | concatenate | bytes 57344 | tf_op jit(solution)/shard_map/concatenate | solution.py:502
  2.1 99.7 %shard_map.181 = bf16[256,512]{1,0:T(8,128)(2,1)} custom-call(bf16[2,128,2048]{2,1,0:T(8,128)(2,1)} %x_ref.1, f32[1,2048]{1,0:T(1,128)} %bitcast.8, bf16[16,896]{1,0:T(8,128)(2,1)} %concatenate.3.w_ref, f32[1,64]{1,0:T(1,128)} %bitcast.12, f32[1,64]{1,0:T(1,128)} %bitcast.13, bf16[4,256]{1,0:T(4,128)(2,1)} %cw_ref.1, bf16[4,64,64]{2,1,0:T(8,128)(2,1)} %dw_ref.1, ...), custom_call_target="tpu_custom_call" | custom-call | tf_op jit(solution)/shard_map/pallas_call | solution.py:453
  101.8 1.7 %copy.21 = bf16[2,128,512]{2,1,0:T(8,128)(2,1)} copy(bf16[2,128,512]{2,1,0:T(8,128)(2,1)} %bitcast.7) | data formatting | bytes 524288
Async XLA Ops:
  0.0 0.7 copy-start

commit v6 on v5

--- a/solution.py
+++ b/solution.py
@@ -339,13 +339,17 @@
         rhs = jnp.concatenate(
             [jnp.concatenate([x[:64] for x in blocks], axis=1), jnp.concatenate(near_gates, axis=1)], axis=0
         )
-        s = jnp.dot(q_ref[b], rhs, preferred_element_type=F32)
-        old = top[b][:, :1]
-        m = jnp.maximum(old, jnp.max(s, axis=1, keepdims=True))
-        p = jnp.exp(s - m).astype(BF16)
         vx = jnp.concatenate([jnp.concatenate([x[64:] for x in blocks], axis=1), ones], axis=0)
-        acc[b] = acc[b] * jnp.exp(old - m) + lax.dot_general(p, vx, NT, preferred_element_type=F32)
-        top[b] = jnp.broadcast_to(m, (rows, 128))
+        half = rows // 2
+        starts = (0, half)
+        scores = [jnp.dot(q_ref[b, at:at + half], rhs, preferred_element_type=F32) for at in starts]
+        for at, s in zip(starts, scores):
+            old = top[b, at:at + half][:, :1]
+            m = jnp.maximum(old, jnp.max(s, axis=1, keepdims=True))
+            p = jnp.exp(s - m).astype(BF16)
+            fresh = lax.dot_general(p, vx, NT, preferred_element_type=F32)
+            acc[b, at:at + half] = acc[b, at:at + half] * jnp.exp(old - m) + fresh
+            top[b, at:at + half] = jnp.broadcast_to(m, (half, 128))
 
     def work(b, *parts):
         near = [j * (16 if b == 0 else 2) < me for j, _ in parts]
@@ -385,11 +389,16 @@
     for s in range(1, 5):
         chain.step_shared(s)
 
-    def merge(j, state):
-        part = st.at[j // 16, lax.rem(j // 2, RING), lax.rem(j, 2)]
-        return part[0] * state + part[1]
-
-    entering = lax.fori_loop(0, me, merge, jnp.zeros((2, 256), F32))
+    places = lax.broadcasted_iota(jnp.int32, (RING, 2, 256), 0) * 16
+    decay, state = jnp.ones((RING, 2, 256), F32), jnp.zeros((RING, 2, 256), F32)
+    for i in range(16):
+        before = places + i < me
+        shrink = jnp.where(before, st[:, i // 2, i % 2, 0], 1.0)
+        state = shrink * state + jnp.where(before, st[:, i // 2, i % 2, 1], 0.0)
+        decay = shrink * decay
+    entering = jnp.zeros((2, 256), F32)
+    for z in range(RING):
+        entering = decay[z] * entering + state[z]
     width = out_ref.shape[1]
     loads[1].wait()
     loads[2].wait()
@@ -427,8 +436,8 @@
 
     products(0, 3)
     sides(1, 3, its)
+    work(1, (keys.back(1, 0, 4), 0), (keys.back(1, 0, 4), 1))
     relay(0, 3)
-    work(1, (keys.back(1, 0, 4), 0), (keys.back(1, 0, 4), 1))
     products(1, 1)
     relay(1, 1)
     for group in (first_w, more_w, keys, chain):

time: 104 us -> 100 us (0.962)
  Pallas kernels: 99.7 us -> 96.3 us
    pallas_call x1, Pallas kernels: 99.7 us -> 96.3 us  [layer(): pl.pallas_call(kernel, out_shape=jax.ShapeDtypeStruct((2 * span, width),...]
where the time goes in v6:
time: 100 us
  Pallas kernels  96.3 us (96%)
  local copies, waits for them, and re-layouts  3.8 us (4%)
    pallas_call x1, Pallas kernels, layer(): pl.pallas_call(kernel, out_shape=jax.ShapeDtypeStruct((2 * span, width),...  96.3 us
    unnamed x3, local copies, waits for them, and re-layouts  2.37 us

profile of v6, /device:TPU:1, one launch (start us, length us, event | category | flops | bytes accessed | tf_op | source)
XLA Modules:
  0.0 100.1 jit_solution(6567105008664150406)
XLA Ops:
  0.0 0.0 copy-start
  0.0 0.7 copy-done
  0.7 1.4 %concatenate.3.w_ref = bf16[16,896]{1,0:T(8,128)(2,1)} concatenate(bf16[16,64]{1,0:T(8,128)(2,1)} %param.22, bf16[16,64]{1,0:T(8,128)(2,1)} %param.23, bf16[16,256]{1,0:T(8,128)(2,1)S(1)} %copy-done, bf16[16,256]{1,0:T(8,128)(2,1)} %param.27, bf16[16,256]{1,0:T(8,128)(2,1)} %param.28), dimensions={1} | concatenate | bytes 57344 | tf_op jit(solution)/shard_map/concatenate | solution.py:511
  2.1 96.3 %shard_map.181 = bf16[256,512]{1,0:T(8,128)(2,1)} custom-call(bf16[2,128,2048]{2,1,0:T(8,128)(2,1)} %x_ref.1, f32[1,2048]{1,0:T(1,128)} %bitcast.8, bf16[16,896]{1,0:T(8,128)(2,1)} %concatenate.3.w_ref, f32[1,64]{1,0:T(1,128)} %bitcast.12, f32[1,64]{1,0:T(1,128)} %bitcast.13, bf16[4,256]{1,0:T(4,128)(2,1)} %cw_ref.1, bf16[4,64,64]{2,1,0:T(8,128)(2,1)} %dw_ref.1, ...), custom_call_target="tpu_custom_call" | custom-call | tf_op jit(solution)/shard_map/pallas_call | solution.py:462
  98.5 1.7 %copy.21 = bf16[2,128,512]{2,1,0:T(8,128)(2,1)} copy(bf16[2,128,512]{2,1,0:T(8,128)(2,1)} %bitcast.7) | data formatting | bytes 524288
Async XLA Ops:
  0.0 0.7 copy-start

commit v7 on v6

--- a/solution.py
+++ b/solution.py
@@ -309,6 +309,7 @@
         ends[0, b:b + 1] = mul[span - 1:]
         ends[1, b:b + 1] = add[span - 1:]
     chain.begin()
+    keys.step(1)
 
     ones_own = jnp.ones((16, span), BF16)
     ones = jnp.ones((16, line), BF16)
@@ -359,7 +360,6 @@
         work(b, *[(keys.back(b, d, s), core) for d in (0, 1)])
 
     mine, its = keys.c, 1 - keys.c
-    keys.step(1)
     keys.own_shared()
     work(0, (keys.z, 0), (keys.z, 1))
     work(1, (keys.y, 0), (keys.y, 1))

time: 100 us -> 102 us (1.020)
  Pallas kernels: 96.3 us -> 97.6 us
    pallas_call x1, Pallas kernels: 96.3 us -> 97.6 us  [layer(): pl.pallas_call(kernel, out_shape=jax.ShapeDtypeStruct((2 * span, width),...]
where the time goes in v7:
time: 102 us; the launch traced here: 101 us
  Pallas kernels  97.6 us (96%)
  local copies, waits for them, and re-layouts  3.8 us (4%)
    pallas_call x1, Pallas kernels, layer(): pl.pallas_call(kernel, out_shape=jax.ShapeDtypeStruct((2 * span, width),...  97.6 us
    unnamed x3, local copies, waits for them, and re-layouts  2.37 us

profile of v7, /device:TPU:1, one launch (start us, length us, event | category | flops | bytes accessed | tf_op | source)
XLA Modules:
  0.0 101.4 jit_solution(11340744834162141796)
XLA Ops:
  0.0 0.0 copy-start
  0.0 0.7 copy-done
  0.7 1.4 %concatenate.3.w_ref = bf16[16,896]{1,0:T(8,128)(2,1)} concatenate(bf16[16,64]{1,0:T(8,128)(2,1)} %param.22, bf16[16,64]{1,0:T(8,128)(2,1)} %param.23, bf16[16,256]{1,0:T(8,128)(2,1)S(1)} %copy-done, bf16[16,256]{1,0:T(8,128)(2,1)} %param.27, bf16[16,256]{1,0:T(8,128)(2,1)} %param.28), dimensions={1} | concatenate | bytes 57344 | tf_op jit(solution)/shard_map/concatenate | solution.py:511
  2.1 97.6 %shard_map.181 = bf16[256,512]{1,0:T(8,128)(2,1)} custom-call(bf16[2,128,2048]{2,1,0:T(8,128)(2,1)} %x_ref.1, f32[1,2048]{1,0:T(1,128)} %bitcast.8, bf16[16,896]{1,0:T(8,128)(2,1)} %concatenate.3.w_ref, f32[1,64]{1,0:T(1,128)} %bitcast.12, f32[1,64]{1,0:T(1,128)} %bitcast.13, bf16[4,256]{1,0:T(4,128)(2,1)} %cw_ref.1, bf16[4,64,64]{2,1,0:T(8,128)(2,1)} %dw_ref.1, ...), custom_call_target="tpu_custom_call" | custom-call | tf_op jit(solution)/shard_map/pallas_call | solution.py:462
  99.7 1.7 %copy.21 = bf16[2,128,512]{2,1,0:T(8,128)(2,1)} copy(bf16[2,128,512]{2,1,0:T(8,128)(2,1)} %bitcast.7) | data formatting | bytes 524288
Async XLA Ops:
  0.0 0.7 copy-start
